TPU v7x, 32 devices: a whole 2x2x4 slice. The times are simulated.
32 devices in a mesh: sp: 8 (over z, x), tp: 4 (over y, core).
Axes of the slice: x: 2, y: 2, z: 4, core: 2. Of those that a mesh axis runs over, the one named last changes fastest.
Arguments:
- latents: bfloat16 [4096, 2048], P(('sp', 'tp')), may hold values from -6 to 6
- context: bfloat16 [512, 2048], P('sp'), may hold values from -6 to 6
- cond: float32 [2048], P('sp'), may hold values from -6 to 6
- ctx_cond: float32 [2048], P('sp'), may hold values from -6 to 6
- mod_weight: float32 [2048, 6144], P('sp', 'tp'), may hold values from -0.125 to 0.125
- query_weight: bfloat16 [2048, 2048], P(None, 'tp'), may hold values from -1 to 1, as said below
- key_matrix: bfloat16 [2048, 1024], P(None, 'tp'), may hold values from -1 to 1, as said below
- value_matrix: bfloat16 [2048, 1024], P(None, 'tp'), may hold values from -0.125 to 0.125
- out_weight: bfloat16 [2048, 2048], P('tp'), may hold values from -0.125 to 0.125
- query_gain: float32 [128], replicated, may hold values from 0.7 to 7
- key_gain: float32 [128], replicated, may hold values from 0.7 to 7
Outputs:
- updated: bfloat16 [4096, 2048], P(('sp', 'tp'))
Inputs may be any that keep to these rules, and one draw needn't show every extreme that they name: `query_weight`: entries of order 2048 to the power -1/2. `key_matrix`: entries of order 2048 to the power -1/2.
All inputs are finite; a program needn't handle non-finite values.
Results may differ from a plain program's by a relative error of at most 0.0085.
The roundings to bfloat16 on the way count: a program that leaves them out, or rounds other values in their place, can miss the bound.
Values may be sent and summed in bfloat16 or wider, within the bound.
A program may use at most 128 MiB of HBM per device.

v0:
```python
import functools
import math

import jax
import jax.numpy as jnp
from jax import lax
from jax.experimental import pallas as pl
from jax.experimental.pallas import tpu as pltpu
from jax.sharding import PartitionSpec as P

GRID_W = 64
NORM_EPS = 1e-06
ROPE_BASE = 10000.0
MESH = pl.DeviceIdType.MESH
BF16 = jnp.bfloat16
F32 = jnp.float32
VMEM_BYTES = 67043328


def row_size(sp_count):
    size = 1
    while 4 * size * size <= sp_count:
        size *= 2
    return size


def tables(positions, head_dim):
    quarter = head_dim // 4
    inv_freq = ROPE_BASE ** (-jnp.arange(quarter, dtype=F32) / quarter)
    where = jnp.stack([positions // GRID_W, positions % GRID_W]).astype(F32)
    angles = where[:, None, :] * inv_freq[None, :, None]
    return jnp.cos(angles), jnp.sin(angles)


def remote(src, dst, send, recv, dev):
    return pltpu.make_async_remote_copy(
        src_ref=src, dst_ref=dst, send_sem=send, recv_sem=recv, device_id=dev, device_id_type=MESH
    )


def front_kernel(
    sp_count, tp_count, head_dim,
    cond_ref, cond_1_ref, mw_hbm, lat_hbm, ctx_ref, wq_hbm, wk_hbm, wv_hbm, qg_ref, kg_ref, cos_ref, sin_ref,
    qt_ref, k_ref, vt_ref, ckv_ref, gate_ref,
    mw, lat, wq, wk, wv, part, tot, mod, xn, load_sem,
    lat_send, lat_recv, part_send, part_recv, tot_send, tot_recv,
    wo_hbm, wo_vm, wo_sem,
):
    s, t = lax.axis_index("sp"), lax.axis_index("tp")
    y, c = t // 2, t % 2
    y_count = tp_count // 2
    partner = y * 2 + 1 - c
    rows = lat.shape[1]
    width = lat.shape[2]
    model_cols = mod.shape[1]

    own = pltpu.make_async_copy(lat_hbm, lat.at[t], load_sem.at[0])
    own.start()
    loads = [
        pltpu.make_async_copy(a, b, load_sem.at[1 + i])
        for i, (a, b) in enumerate(((mw_hbm, mw), (wq_hbm, wq), (wk_hbm, wk), (wv_hbm, wv)))
    ]
    for one in loads:
        one.start()

    pltpu.make_async_copy(wo_hbm, wo_vm, wo_sem.at[0]).start()

    barrier = pltpu.get_barrier_semaphore()
    for j in range(1, sp_count):
        pl.semaphore_signal(barrier, inc=1, device_id=((s + j) % sp_count, t), device_id_type=MESH)
    for j in range(1, tp_count):
        pl.semaphore_signal(barrier, inc=1, device_id=(s, (t + j) % tp_count), device_id_type=MESH)
    pl.semaphore_wait(barrier, sp_count + tp_count - 2)

    own.wait()
    sends = []
    for j in range(1, y_count):
        peer = ((y + j) % y_count) * 2 + c
        sends.append(remote(lat.at[t], lat.at[t], lat_send.at[j], lat_recv.at[t], (s, peer)))
    sends.append(remote(lat.at[t], lat.at[t], lat_send.at[0], lat_recv.at[t], (s, partner)))
    for one in sends:
        one.start()

    loads[0].wait()
    lines = lax.broadcasted_iota(jnp.int32, (8, cond_ref.shape[1]), 0)
    cond = jnp.where(lines == 0, cond_ref[...], jnp.where(lines == 1, cond_1_ref[...], 0.0))
    cond = cond * jax.nn.sigmoid(cond)
    part[s] = jnp.dot(
        cond, mw[...], precision=lax.Precision.HIGHEST, preferred_element_type=F32
    )[:2]
    more = [
        remote(part.at[s], part.at[s], part_send.at[j], part_recv.at[s], ((s + j) % sp_count, t))
        for j in range(1, sp_count)
    ]
    for one in more:
        one.start()
    for j in range(1, sp_count):
        src = (s + j) % sp_count
        remote(part.at[src], part.at[src], part_send.at[0], part_recv.at[src], (s, t)).wait_recv()
    total = part[0]
    for j in range(1, sp_count):
        total = total + part[j]
    tot[t] = total
    last = [
        remote(tot.at[t], tot.at[t], tot_send.at[j], tot_recv.at[t], (s, (t + j) % tp_count))
        for j in range(1, tp_count)
    ]
    for one in last:
        one.start()
    for j in range(1, tp_count):
        src = (t + j) % tp_count
        remote(tot.at[src], tot.at[src], tot_send.at[0], tot_recv.at[src], (s, t)).wait_recv()
    cols = model_cols // tp_count
    for j in range(tp_count):
        mod[:, j * cols : (j + 1) * cols] = tot[j]
    gate_ref[...] = mod[0:1, 2 * width :]

    def modulate(x, r):
        x = x.astype(F32)
        scaled = x * lax.rsqrt(jnp.mean(x * x, axis=-1, keepdims=True) + NORM_EPS)
        shift, scale = mod[r : r + 1, :width], mod[r : r + 1, width : 2 * width]
        return (scaled * (1.0 + scale) + shift).astype(BF16)

    for one in loads[1:]:
        one.wait()

    cn = modulate(ctx_ref[...], 1)
    kc = jnp.dot(cn, wk[...], preferred_element_type=F32)
    vc = jnp.dot(cn, wv[...], preferred_element_type=F32)
    for h in range(kc.shape[1] // head_dim):
        kh = kc[:, h * head_dim : (h + 1) * head_dim]
        kh = kh * lax.rsqrt(jnp.mean(kh * kh, axis=-1, keepdims=True) + NORM_EPS) * kg_ref[...]
        ckv_ref[h, 0] = kh.astype(BF16)
        ckv_ref[h, 1] = vc[:, h * head_dim : (h + 1) * head_dim].astype(BF16)

    q4 = head_dim // 4
    qgain, kgain = qg_ref[...], kg_ref[...]

    def turn(yt, cos, sin):
        out = []
        for n in range(2):
            a = yt[2 * n * q4 : (2 * n + 1) * q4]
            b = yt[(2 * n + 1) * q4 : (2 * n + 2) * q4]
            out += [a * cos[n] - b * sin[n], b * cos[n] + a * sin[n]]
        return jnp.concatenate(out, axis=0)

    def unit(yh, gain):
        return yh * lax.rsqrt(jnp.mean(yh * yh, axis=-1, keepdims=True) + NORM_EPS) * gain

    span = 2 * rows
    relays = []
    for j in range(y_count):
        yy = (y + j) % y_count
        if j > 0:
            src = yy * 2 + c
            remote(lat.at[src], lat.at[src], lat_send.at[0], lat_recv.at[src], (s, t)).wait_recv()
            one = remote(
                lat.at[src], lat.at[src], lat_send.at[y_count - 1 + j], lat_recv.at[src], (s, partner)
            )
            one.start()
            relays.append(one)
        other = yy * 2 + 1 - c
        remote(lat.at[other], lat.at[other], lat_send.at[0], lat_recv.at[other], (s, t)).wait_recv()
        for i in range(2):
            xn[i * rows : (i + 1) * rows, :] = modulate(lat[yy * 2 + i], 0)
        x = xn[...]
        at = pl.ds(pl.multiple_of(yy * span, span), span)
        cos, sin = cos_ref[:, :, at], sin_ref[:, :, at]
        for w, kind in ((wq, 0), (wk, 1), (wv, 2)):
            step = min(2 * head_dim, w.shape[1])
            for n in range(0, w.shape[1], step):
                full = jnp.dot(x, w[:, n : n + step], preferred_element_type=F32)
                for m in range(0, step, head_dim):
                    h = (n + m) // head_dim
                    yh = full[:, m : m + head_dim]
                    if kind == 0:
                        qt_ref[h, :, at] = turn(unit(yh, qgain).T, cos, sin).astype(BF16)
                    elif kind == 1:
                        k_ref[h, at, :] = turn(unit(yh, kgain).T, cos, sin).T.astype(BF16)
                    else:
                        vt_ref[h, :, at] = yh.T.astype(BF16)
    for one in sends + more + last + relays:
        one.wait_send()


def attend_kernel(
    sp_count, x_count, group, lift,
    k_hbm, vt_hbm, ckv_hbm, qt_ref,
    out_ref,
    kb, vb, cb, top, tot, acc, load_sem, send_sem, recv_sem,
):
    s, t = lax.axis_index("sp"), lax.axis_index("tp")
    z, x = s // x_count, s % x_count
    z_count = sp_count // x_count
    heads, head_dim, rows = qt_ref.shape
    kv_heads = heads // group
    factor = head_dim ** (-0.5) * math.log2(math.e)

    loads = [
        pltpu.make_async_copy(a, b, load_sem.at[i])
        for i, (a, b) in enumerate(
            (
                (ckv_hbm, cb.at[s]),
                (k_hbm, kb.at[s]),
                (vt_hbm, vb.at[s]),
            )
        )
    ]
    for one in loads:
        one.start()
    targets = []
    for sign in (1, -1):
        ok = (z + sign >= 0) & (z + sign < z_count)
        peer = ((z + sign + z_count) % z_count) * x_count + x
        targets.append((ok, peer))

    top[...] = jnp.full_like(top, -1e30)
    tot[...] = jnp.zeros_like(tot)
    acc[...] = jnp.zeros_like(acc)
    for one in loads:
        one.wait()

    bufs = (cb, kb, vb)

    def copies(src, way, peer):
        return [
            remote(b.at[src], b.at[src], send_sem.at[i, src, way], recv_sem.at[i, src], (peer, t))
            for i, b in enumerate(bufs)
        ]

    def source(k):
        low = jnp.minimum(z, z_count - 1 - z)
        both = k <= 2 * low
        dist = jnp.where(both, (k + 1) // 2, k - low)
        up = jnp.where(both, k % 2 == 1, z < z_count - 1 - z)
        return jnp.where(up, z + dist, z - dist)

    def update(i, keys, values_t, bias):
        sc = jnp.dot(keys, qt_ref[i], preferred_element_type=F32) * factor
        if bias != 0.0:
            sc = sc + bias
        old = top[i]
        new = jnp.maximum(old, jnp.max(sc, axis=0, keepdims=True))
        p = jnp.exp2(sc - new)
        f = jnp.exp2(old - new)
        top[i] = new
        tot[i] = tot[i] * f + jnp.sum(p, axis=0, keepdims=True)
        acc[i] = acc[i] * f + jnp.dot(values_t, p.astype(BF16), preferred_element_type=F32)

    def block(src):
        def head(i, carry):
            h = i // group
            update(i, kb[src, h], vb[src, h], 0.0)
            return carry

        lax.fori_loop(0, heads, head, 0)

    def wait_from(src):
        for one in copies(src, 0, s):
            one.wait_recv()

    def step(k, carry):
        zz = source(k)
        src = zz * x_count + x

        @pl.when(k > 0)
        def _():
            wait_from(src)

        for way, (ok, peer) in enumerate(targets):
            mine = zz <= z if way == 0 else zz >= z

            @pl.when(ok & mine)
            def _():
                for one in copies(src, way, peer):
                    one.start()

        for j in range(1, x_count):
            for one in copies(src, 1 + j, z * x_count + (x + j) % x_count):
                one.start()
        block(src)

        @pl.when(k > 0)
        def _():
            before = source(k - 1)
            for j in range(1, x_count):
                old = before * x_count + (x + j) % x_count
                wait_from(old)
                block(old)

        return carry

    lax.fori_loop(0, z_count, step, 0)
    final = source(z_count - 1)
    ends = [final * x_count + (x + j) % x_count for j in range(1, x_count)]
    for src in ends:
        copies(src, 0, s)[0].wait_recv()
    for i in range(heads):
        h = i // group
        keys = jnp.concatenate([cb[j, h, 0] for j in range(sp_count)], axis=0)
        vals = jnp.concatenate([cb[j, h, 1] for j in range(sp_count)], axis=0)
        update(i, keys, vals.astype(F32).T.astype(BF16), lift * math.log2(math.e))
    for src in ends:
        for one in copies(src, 0, s)[1:]:
            one.wait_recv()
        block(src)
    for i in range(heads):
        out_ref[:, i * head_dim : (i + 1) * head_dim] = (acc[i] / tot[i]).T.astype(BF16)

    def drain(k, carry):
        zz = source(k)
        src = zz * x_count + x
        for way, (ok, peer) in enumerate(targets):
            mine = zz <= z if way == 0 else zz >= z

            @pl.when(ok & mine)
            def _():
                for one in copies(src, way, peer):
                    one.wait_send()

        for j in range(1, x_count):
            for one in copies(src, 1 + j, z * x_count + (x + j) % x_count):
                one.wait_send()
        return carry

    lax.fori_loop(0, z_count, drain, 0)


def pair_kernel(
    sp_count, x_count, group, lift,
    k_hbm, vt_hbm, ckv_hbm, qt_ref,
    out_ref,
    kb, vb, cb, top, tot, acc, load_sem, qb, ab, send_sem, recv_sem, swap_sem,
):
    s, t = lax.axis_index("sp"), lax.axis_index("tp")
    z, x = s // x_count, s % x_count
    z_count = sp_count // x_count
    heads, head_dim, rows = qt_ref.shape
    factor = head_dim ** (-0.5) * math.log2(math.e)
    mine = z % 2
    mate = (z + 1 - 2 * mine) * x_count + x

    bufs = (cb, kb, vb)
    loads = [
        pltpu.make_async_copy(a, b.at[s], load_sem.at[i])
        for i, (a, b) in enumerate(zip((ckv_hbm, k_hbm, vt_hbm), bufs))
    ]
    for one in loads:
        one.start()
    swap_q = remote(
        qt_ref.at[pl.ds((1 - mine) * group, group)], qb.at[0],
        swap_sem.at[0], swap_sem.at[1], (mate, t),
    )
    swap_q.start()
    qb[1] = qt_ref[pl.ds(mine * group, group)]
    top[...] = jnp.full_like(top, -1e30)
    tot[...] = jnp.zeros_like(tot)
    acc[...] = jnp.zeros_like(acc)
    for one in loads:
        one.wait()

    def copy(i, src, h, way, peer):
        b = bufs[i]
        return remote(
            b.at[src, h], b.at[src, h], send_sem.at[i, way], recv_sem.at[i, src], (peer, t)
        )

    def source(k):
        low = jnp.minimum(z, z_count - 1 - z)
        both = k <= 2 * low
        dist = jnp.where(both, (k + 1) // 2, k - low)
        up = jnp.where(both, k % 2 == 1, z < z_count - 1 - z)
        return jnp.where(up, z + dist, z - dist)

    def line(act):
        for dist in range(1, z_count):
            for sign in (1, -1):
                there = z + sign * dist

                @pl.when((there >= 0) & (there < z_count))
                def _():
                    to = (there + z_count) % z_count
                    for i in range(3):
                        act(copy(i, s, to % 2, to, to * x_count + x))

    def across(k, act):
        zz = source(k)
        src = zz * x_count + x
        for i in range(3):
            if act is None:

                @pl.when(k > 0)
                def _():
                    copy(i, src, mine, 0, s).wait_recv()

            for j in range(1, x_count):
                way = z_count + zz * (x_count - 1) + j - 1
                one = copy(i, src, mine, way, z * x_count + (x + j) % x_count)
                one.start() if act is None else act(one)

    def update(i, queries, keys, values_t, bias):
        sc = jnp.dot(keys, queries, preferred_element_type=F32) * factor
        if bias != 0.0:
            sc = sc + bias
        old = top[i]
        new = jnp.maximum(old, jnp.max(sc, axis=0, keepdims=True))
        p = jnp.exp2(sc - new)
        f = jnp.exp2(old - new)
        top[i] = new
        tot[i] = tot[i] * f + jnp.sum(p, axis=0, keepdims=True)
        acc[i] = acc[i] * f + jnp.dot(values_t, p.astype(BF16), preferred_element_type=F32)

    def block(src):
        def tile(i, carry):
            update(i, qb[i // group, i % group], kb[src, mine], vb[src, mine], 0.0)
            return carry

        lax.fori_loop(0, 2 * group, tile, 0)

    def step(k, carry):
        across(k, None)

        @pl.when(k == 0)
        def _():
            swap_q.wait_recv()

        block(source(k) * x_count + x)

        @pl.when(k > 0)
        def _():
            before = source(k - 1)
            for j in range(1, x_count):
                old = before * x_count + (x + j) % x_count
                for i in range(3):
                    copy(i, old, mine, 0, s).wait_recv()
                block(old)

        return carry

    line(lambda one: one.start())
    lax.fori_loop(0, z_count, step, 0)
    final = source(z_count - 1)
    ends = [final * x_count + (x + j) % x_count for j in range(1, x_count)]
    for src in ends:
        copy(0, src, mine, 0, s).wait_recv()
    keys = jnp.concatenate([cb[j, mine, 0] for j in range(sp_count)], axis=0)
    vals = jnp.concatenate([cb[j, mine, 1] for j in range(sp_count)], axis=0)
    vals = vals.astype(F32).T.astype(BF16)
    span = group * head_dim
    swap_a = remote(ab.at[0], ab.at[1], swap_sem.at[2], swap_sem.at[3], (mate, t))
    for who in range(2):
        for g in range(group):
            update(who * group + g, qb[who, g], keys, vals, lift * math.log2(math.e))
        for src in ends:
            if who == 0:
                for i in (1, 2):
                    copy(i, src, mine, 0, s).wait_recv()
            for g in range(group):
                update(who * group + g, qb[who, g], kb[src, mine], vb[src, mine], 0.0)
        for g in range(group):
            i = who * group + g
            done = (acc[i] / tot[i]).T.astype(BF16)
            if who == 0:
                ab[0, :, g * head_dim : (g + 1) * head_dim] = done
            else:
                at = pl.ds(pl.multiple_of(mine * span + g * head_dim, head_dim), head_dim)
                out_ref[:, at] = done
        if who == 0:
            swap_a.start()

    def drain(k, carry):
        across(k, lambda one: one.wait_send())
        return carry

    lax.fori_loop(0, z_count, drain, 0)
    line(lambda one: one.wait_send())
    swap_a.wait_recv()
    out_ref[:, pl.ds(pl.multiple_of((1 - mine) * span, head_dim), span)] = ab[1]
    swap_q.wait_send()
    swap_a.wait_send()


def mix_kernel(
    tp_count, chunks,
    att_ref, wo_hbm, wo_ref, wo_sem, lat_ref, gate_ref,
    out_ref,
    core_out, core_in, mesh_out, mesh_in, mixed, core_send, core_recv, mesh_send, mesh_recv,
):
    s, t = lax.axis_index("sp"), lax.axis_index("tp")
    y, c = t // 2, t % 2
    y_count = tp_count // 2
    partner = y * 2 + 1 - c
    rows, width = lat_ref.shape
    step = width // chunks
    peers = [((y + j) % y_count) * 2 + c for j in range(1, y_count)]
    pltpu.make_async_copy(wo_hbm, wo_ref, wo_sem.at[0]).wait()

    def piece(n, j, cc):
        yy = (y + j) % y_count
        at = pl.ds(pl.multiple_of((yy * 2 + cc) * rows, rows), rows)
        return jnp.dot(
            att_ref[at, :], wo_ref[:, n * step : (n + 1) * step], preferred_element_type=F32
        )

    order = list(range(1, y_count)) + [0]
    cores = [
        remote(core_out.at[n], core_in.at[n], core_send.at[n], core_recv.at[n], (s, partner))
        for n in range(chunks)
    ]
    sent = []
    for n in range(chunks + 1):
        if n < chunks:
            for j in order:
                core_out[n, j] = piece(n, j, 1 - c).astype(BF16)
            cores[n].start()
        if n == 0:
            continue
        m = n - 1
        own = [piece(m, j, c) for j in order]
        cores[m].wait_recv()
        for j, value in zip(order, own):
            value = value + core_in[m, j].astype(F32)
            if j == 0:
                mixed[m] = value
            else:
                mesh_out[m, j - 1] = value.astype(BF16)
                one = remote(
                    mesh_out.at[m, j - 1], mesh_in.at[m, j - 1], mesh_send.at[m, j - 1],
                    mesh_recv.at[m, j - 1], (s, peers[j - 1]),
                )
                one.start()
                sent.append(one)
    for one in sent:
        one.wait_recv()
    square = jnp.zeros((rows, 1), F32)
    for n in range(chunks):
        value = mixed[n]
        for j in range(1, y_count):
            value = value + mesh_in[n, j - 1].astype(F32)
        mixed[n] = value
        square = square + jnp.sum(value * value, axis=-1, keepdims=True)
    inv = lax.rsqrt(square / width + NORM_EPS)
    for n in range(chunks):
        at = slice(n * step, (n + 1) * step)
        out_ref[:, at] = (
            lat_ref[:, at].astype(F32) + gate_ref[:, at] * (mixed[n] * inv)
        ).astype(BF16)
    for one in sent + cores:
        one.wait_send()


def whole_kernel(sp_count, tp_count, x_count, head_dim, group, lift, chunks, paired, counts, *refs):
    (
        cond, cond_1, mw, lat, ctx, wq, wk, wv, qg, kg, cos, sin, wo, lat_rows,
        out, qt, k, vt, ckv, gate, att, wo_vm, wo_sem, *rest,
    ) = refs
    front, middle, last = counts
    front_scratch, middle_scratch = rest[:front], rest[front : front + middle]
    front_kernel(
        sp_count, tp_count, head_dim, cond, cond_1, mw, lat, ctx, wq, wk, wv, qg, kg, cos, sin,
        qt, k, vt, ckv, gate, *front_scratch, wo, wo_vm, wo_sem,
    )
    attention = pair_kernel if paired else attend_kernel
    attention(sp_count, x_count, group, lift, k, vt, ckv, qt, att, *middle_scratch)
    mix_kernel(
        tp_count, chunks, att, wo, wo_vm, wo_sem, lat_rows, gate, out, *rest[front + middle :]
    )


ANY = pl.BlockSpec(memory_space=pl.ANY)
VM = pl.BlockSpec(memory_space=pltpu.VMEM)
DMA = pltpu.SemaphoreType.DMA


def body(
    latents,
    context,
    cond,
    ctx_cond,
    mod_weight,
    query_weight,
    key_matrix,
    value_matrix,
    out_weight,
    query_gain,
    key_gain,
):
    sp_count, tp_count = lax.axis_size("sp"), lax.axis_size("tp")
    x_count = row_size(sp_count)
    rows, width = latents.shape
    ctx_rows = context.shape[0]
    head_dim = query_gain.shape[0]
    heads = query_weight.shape[1] // head_dim
    kv_heads = key_matrix.shape[1] // head_dim
    all_rows = rows * tp_count
    mod_cols = mod_weight.shape[1]
    positions = lax.axis_index("sp") * all_rows + jnp.arange(all_rows, dtype=jnp.int32)
    cos, sin = tables(positions, head_dim)
    lift = math.log(sp_count * all_rows / (2.0 * sp_count * ctx_rows))
    group = heads // kv_heads
    paired = kv_heads == 2 and (sp_count // x_count) % 2 == 0
    chunks = 4
    y_count = tp_count // 2
    step = width // chunks
    far = max(y_count - 1, 1)
    shared = [
        pltpu.VMEM((heads, head_dim, all_rows), BF16),
        pltpu.VMEM((kv_heads, all_rows, head_dim), BF16),
        pltpu.VMEM((kv_heads, head_dim, all_rows), BF16),
        pltpu.VMEM((kv_heads, 2, ctx_rows, head_dim), BF16),
        pltpu.VMEM((1, width), F32),
        pltpu.VMEM((all_rows, heads * head_dim), BF16),
        pltpu.VMEM(out_weight.shape, BF16),
        DMA((1,)),
    ]
    front = [
        pltpu.VMEM(mod_weight.shape, F32),
        pltpu.VMEM((tp_count, rows, width), BF16),
        pltpu.VMEM(query_weight.shape, BF16),
        pltpu.VMEM(key_matrix.shape, BF16),
        pltpu.VMEM(value_matrix.shape, BF16),
        pltpu.VMEM((sp_count, 2, mod_cols), F32),
        pltpu.VMEM((tp_count, 2, mod_cols), F32),
        pltpu.VMEM((2, mod_cols * tp_count), F32),
        pltpu.VMEM((2 * rows, width), BF16),
        DMA((5,)),
        DMA((tp_count,)),
        DMA((tp_count,)),
        DMA((sp_count,)),
        DMA((sp_count,)),
        DMA((tp_count,)),
        DMA((tp_count,)),
    ]
    middle = [
        pltpu.VMEM((sp_count, kv_heads, all_rows, head_dim), BF16),
        pltpu.VMEM((sp_count, kv_heads, head_dim, all_rows), BF16),
        pltpu.VMEM((sp_count, kv_heads, 2, ctx_rows, head_dim), BF16),
        pltpu.VMEM((heads, 1, all_rows), F32),
        pltpu.VMEM((heads, 1, all_rows), F32),
        pltpu.VMEM((heads, head_dim, all_rows), F32),
        DMA((3,)),
    ]
    if paired:
        middle += [
            pltpu.VMEM((2, group, head_dim, all_rows), BF16),
            pltpu.VMEM((2, all_rows, group * head_dim), BF16),
            DMA((3, sp_count)),
            DMA((3, sp_count)),
            DMA((4,)),
        ]
    else:
        middle += [DMA((3, sp_count, x_count + 1)), DMA((3, sp_count))]
    last = [
        pltpu.VMEM((chunks, y_count, rows, step), BF16),
        pltpu.VMEM((chunks, y_count, rows, step), BF16),
        pltpu.VMEM((chunks, far, rows, step), BF16),
        pltpu.VMEM((chunks, far, rows, step), BF16),
        pltpu.VMEM((chunks, rows, step), F32),
        DMA((chunks,)),
        DMA((chunks,)),
        DMA((chunks, far)),
        DMA((chunks, far)),
    ]
    counts = (len(front), len(middle), len(last))
    return pl.pallas_call(
        functools.partial(
            whole_kernel, sp_count, tp_count, x_count, head_dim, group, lift, chunks, paired, counts
        ),
        out_shape=jax.ShapeDtypeStruct((rows, width), BF16),
        in_specs=[VM, VM, ANY, ANY, VM, ANY, ANY, ANY, VM, VM, VM, VM, ANY, VM],
        out_specs=VM,
        scratch_shapes=shared + front + middle + last,
        compiler_params=pltpu.CompilerParams(
            collective_id=0, has_side_effects=True, vmem_limit_bytes=VMEM_BYTES
        ),
        name="whole",
    )(
        cond[None], ctx_cond[None], mod_weight, latents, context, query_weight, key_matrix, value_matrix,
        query_gain[None], key_gain[None], cos, sin, out_weight, latents,
    )


def solution(mesh):
    placed = (
        P(("sp", "tp"), None),
        P("sp", None),
        P("sp"),
        P("sp"),
        P("sp", "tp"),
        P(None, "tp"),
        P(None, "tp"),
        P(None, "tp"),
        P("tp", None),
        P(),
        P(),
    )
    return jax.shard_map(
        body, mesh=mesh, in_specs=placed, out_specs=P(("sp", "tp"), None), check_vma=False
    )
```

profile of v0, /device:TPU:1, one launch (start us, length us, event | category | flops | bytes accessed | tf_op | source)
XLA Modules:
  0.0 91.7 jit_solution(11282206700672822871)
XLA Ops:
  0.1 1.2 %multiply_sine_fusion = (f32[2,32,512]{2,1,0:T(8,128)}, f32[2,32,512]{2,1,0:T(8,128)}) fusion(f32[32]{0:T(128)S(1)} %multiply_power_fusion, f32[2,512]{1,0:T(2,128)S(1)} %add_convert_fusion), kind=kLoop, calls=%fused_computation | loop fusion | flops 32768 | bytes 266368 | tf_op jit(solution)/shard_map/sin | solution.py:32
  1.3 88.5 %whole.1 = bf16[128,2048]{1,0:T(8,128)(2,1)} custom-call(f32[1,256]{1,0:T(1,128)} %bitcast.4, f32[1,256]{1,0:T(1,128)} %bitcast.5, f32[256,1536]{1,0:T(8,128)} %refs_2_.1, bf16[128,2048]{1,0:T(8,128)(2,1)} %refs_13_.1, bf16[64,2048]{1,0:T(8,128)(2,1)} %refs_4_.1, bf16[2048,512]{1,0:T(8,128)(2,1)} %refs_5_.1, bf16[2048,256]{1,0:T(8,128)(2,1)} %refs_6_.1, ...), custom_call_target="tpu_custom_call" | custom-call | tf_op jit(solution)/shard_map/whole/pallas_call | solution.py:665
  89.8 1.9 %copy.13 = bf16[128,2048]{1,0:T(8,128)(2,1)} copy(bf16[128,2048]{1,0:T(8,128)(2,1)} %whole.1) | data formatting | bytes 1048576
  (3 shorter events, 0.0 us)
where the time goes:
time: 92.9 us; the launch traced here: 91.7 us
  Pallas kernels  88.5 us (95%)
  local copies, waits for them, and re-layouts  1.88 us (2%)
  other arithmetic  1.28 us (1%)
    pallas_call x1, Pallas kernels, body(): pl.pallas_call(functools.partial(whole_kernel, sp_count, tp_count, x_coun...  88.5 us
    unnamed x1, local copies, waits for them, and re-layouts  1.88 us

commit v1 on v0

--- a/solution.py
+++ b/solution.py
@@ -326,158 +326,434 @@
     lax.fori_loop(0, z_count, drain, 0)
 
 
-def pair_kernel(
-    sp_count, x_count, group, lift,
-    k_hbm, vt_hbm, ckv_hbm, qt_ref,
-    out_ref,
-    kb, vb, cb, top, tot, acc, load_sem, qb, ab, send_sem, recv_sem, swap_sem,
-):
+def quad_kernel(sp_count, head_dim, lift, chunks, *refs):
+    (
+        cond_ref, cond_1_ref, mw_hbm, lat_hbm, ctx_hbm, wq_hbm, wk_hbm, wv_hbm, qg_ref, kg_ref,
+        cos_hbm, sin_hbm, wo_hbm,
+        out_ref,
+        mw, lat, ctx, wq, wk, wv, wo, cos_ref, sin_ref, part, tot, mod, xn,
+        qt, kk, vt, ckv, qb, kb, vb, cb, top, ttl, acc, stats, stats_in, acc_in,
+        score, prob, fade, ob, att, core_out, core_in, mesh_out, mesh_in, mixed,
+        load_sem, lat_send, lat_recv, part_send, part_recv, tot_send, tot_recv,
+        kv_send, kv_recv, c_send, c_recv, q_send, q_recv, relay_send,
+        a_send, a_recv, s_sem, o_send, o_recv, core_send, core_recv, mesh_send, mesh_recv,
+    ) = refs
     s, t = lax.axis_index("sp"), lax.axis_index("tp")
-    z, x = s // x_count, s % x_count
-    z_count = sp_count // x_count
-    heads, head_dim, rows = qt_ref.shape
-    factor = head_dim ** (-0.5) * math.log2(math.e)
-    mine = z % 2
-    mate = (z + 1 - 2 * mine) * x_count + x
-
-    bufs = (cb, kb, vb)
-    loads = [
-        pltpu.make_async_copy(a, b.at[s], load_sem.at[i])
-        for i, (a, b) in enumerate(zip((ckv_hbm, k_hbm, vt_hbm), bufs))
-    ]
+    y, c = t // 2, t % 2
+    z, x = s // 2, s % 2
+    z_count = sp_count // 2
+    quads = z_count // 2
+    quad, low = z // 2, z % 2
+    place = low * 2 + x
+    partner, across = y * 2 + 1 - c, (1 - y) * 2 + c
+    target = (z + x) % 2
+    owner = low == c
+    rows, width = lat.shape[1], lat.shape[2]
+    all_rows = 4 * rows
+    span = 2 * rows
+    first = max(rows * 3 // 128 * 16, 16)
+
+    load_pairs = (
+        (lat_hbm, lat.at[t]), (mw_hbm, mw), (wk_hbm, wk), (wv_hbm, wv), (wq_hbm, wq), (ctx_hbm, ctx),
+        (cos_hbm, cos_ref), (sin_hbm, sin_ref), (wo_hbm, wo),
+    )
+    loads = [pltpu.make_async_copy(a, b, load_sem.at[i]) for i, (a, b) in enumerate(load_pairs)]
     for one in loads:
         one.start()
-    swap_q = remote(
-        qt_ref.at[pl.ds((1 - mine) * group, group)], qb.at[0],
-        swap_sem.at[0], swap_sem.at[1], (mate, t),
-    )
-    swap_q.start()
-    qb[1] = qt_ref[pl.ds(mine * group, group)]
-    top[...] = jnp.full_like(top, -1e30)
-    tot[...] = jnp.zeros_like(tot)
-    acc[...] = jnp.zeros_like(acc)
-    for one in loads:
+
+    barrier = pltpu.get_barrier_semaphore()
+    for j in range(sp_count):
+        for k in range(2):
+            if j + k > 0:
+                dev = ((s + j) % sp_count, y * 2 + (c + k) % 2)
+                pl.semaphore_signal(barrier, inc=1, device_id=dev, device_id_type=MESH)
+    for k in range(2):
+        dev = (s, (1 - y) * 2 + (c + k) % 2)
+        pl.semaphore_signal(barrier, inc=1, device_id=dev, device_id_type=MESH)
+
+    loads[1].wait()
+    lines = lax.broadcasted_iota(jnp.int32, (8, cond_ref.shape[1]), 0)
+    cond = jnp.where(lines == 0, cond_ref[...], jnp.where(lines == 1, cond_1_ref[...], 0.0))
+    cond = cond * jax.nn.sigmoid(cond)
+    part[s] = jnp.dot(
+        cond, mw[...], precision=lax.Precision.HIGHEST, preferred_element_type=F32
+    )[:2]
+    loads[0].wait()
+    pl.semaphore_wait(barrier, 2 * sp_count + 1)
+
+    sends = [
+        remote(part.at[s], part.at[s], part_send.at[j], part_recv.at[s], ((s + j) % sp_count, t))
+        for j in range(1, sp_count)
+    ]
+    sends.append(remote(lat.at[t], lat.at[t], lat_send.at[2], lat_recv.at[2], (s, partner)))
+    pieces = (pl.ds(0, first), pl.ds(first, rows - first))
+    halves = [
+        remote(lat.at[t, at], lat.at[t, at], lat_send.at[i], lat_recv.at[i], (s, across))
+        for i, at in enumerate(pieces)
+    ]
+    for one in sends + halves[:1]:
+        one.start()
+    for j in range(1, sp_count):
+        src = (s + j) % sp_count
+        remote(part.at[src], part.at[src], part_send.at[0], part_recv.at[src], (s, partner)).wait_recv()
+    total = part[0]
+    for j in range(1, sp_count):
+        total = total + part[j]
+    tot[t] = total
+    last = [
+        remote(tot.at[t], tot.at[t], tot_send.at[j], tot_recv.at[t], (s, (t + j) % 4))
+        for j in range(1, 4)
+    ]
+    for one in last + halves[1:]:
+        one.start()
+    sends += last + halves
+    for j in range(1, 4):
+        src = (t + j) % 4
+        remote(tot.at[src], tot.at[src], tot_send.at[0], tot_recv.at[src], (s, partner)).wait_recv()
+    cols = tot.shape[2]
+    for j in range(4):
+        mod[:, j * cols : (j + 1) * cols] = tot[j]
+
+    def relay_rows(i):
+        at = pieces[i]
+        remote(lat.at[across, at], lat.at[across, at], lat_send.at[0], lat_recv.at[i], (s, partner)).wait_recv()
+        one = remote(
+            lat.at[across, at], lat.at[across, at], lat_send.at[3 + i], lat_recv.at[3 + i], (s, partner)
+        )
+        one.start()
+        sends.append(one)
+
+    def modulate(value, r):
+        value = value.astype(F32)
+        scaled = value * lax.rsqrt(jnp.mean(value * value, axis=-1, keepdims=True) + NORM_EPS)
+        shift, scale = mod[r : r + 1, :width], mod[r : r + 1, width : 2 * width]
+        return (scaled * (1.0 + scale) + shift).astype(BF16)
+
+    q4 = head_dim // 4
+    qgain = qg_ref[...] * (head_dim ** (-0.5) * math.log2(math.e))
+    kgain = kg_ref[...]
+
+    def turn(yt, cos, sin):
+        out = []
+        for n in range(2):
+            a = yt[2 * n * q4 : (2 * n + 1) * q4]
+            b = yt[(2 * n + 1) * q4 : (2 * n + 2) * q4]
+            out += [a * cos[n] - b * sin[n], b * cos[n] + a * sin[n]]
+        return jnp.concatenate(out, axis=0)
+
+    def unit(yh, gain):
+        return yh * lax.rsqrt(jnp.mean(yh * yh, axis=-1, keepdims=True) + NORM_EPS) * gain
+
+    def column(yy):
+        return pl.ds(pl.multiple_of(yy * span, span), span)
+
+    def dest(i, n):
+        to = (((quad + n) % quads) * 2 + c) * 2 + i
+        here = (to == s) & (target == c)
+        return to, here
+
+    def send_kv(ph, act):
+        at = column((y + ph) % 2)
+        for n in range(quads):
+            for i in range(2):
+                to, here = dest(i, n)
+                for kind, src, dst in (
+                    (0, kk.at[i, at], kb.at[z, at]), (1, vt.at[i, :, at], vb.at[z, :, at]),
+                ):
+
+                    @pl.when(jnp.logical_not(here))
+                    def _():
+                        act(remote(
+                            src, dst, kv_send.at[kind, ph, n, i], kv_recv.at[kind, ph, z],
+                            (to, y * 2 + target),
+                        ))
+
+    def send_ctx(act):
+        for n in range(quads):
+            for i in range(2):
+                to, here = dest(i, n)
+
+                @pl.when(jnp.logical_not(here))
+                def _():
+                    act(remote(
+                        ckv.at[i], cb.at[z], c_send.at[n, i], c_recv.at[z], (to, y * 2 + target)
+                    ))
+
+    def send_q(ph, act):
+        at = column((y + ph) % 2)
+        for i in range(2):
+            to = (quad * 2 + c) * 2 + i
+            for g in range(2):
+                mine = (to == s) & (g == c)
+                src = qt.at[i * 2 + g, :, at]
+
+                @pl.when(mine)
+                def _():
+                    act(remote(
+                        src, qb.at[0, place, :, at], q_send.at[ph, i, g], q_recv.at[0, place, ph],
+                        (s, partner),
+                    ))
+
+                @pl.when(jnp.logical_not(mine))
+                def _():
+                    act(remote(
+                        src, qb.at[1, place, :, at], q_send.at[ph, i, g], q_recv.at[1, place, ph],
+                        (to, y * 2 + g),
+                    ))
+
+    def start(one):
+        one.start()
+
+    def project(ph):
+        yy = (y + ph) % 2
+        for i in range(2):
+            xn[i * rows : (i + 1) * rows, :] = modulate(lat[yy * 2 + i], 0)
+        value = xn[...]
+        at = column(yy)
+        cos, sin = cos_ref[:, :, at], sin_ref[:, :, at]
+        full = jnp.dot(value, wk[...], preferred_element_type=F32)
+        for h in range(2):
+            yh = full[:, h * head_dim : (h + 1) * head_dim]
+            kk[h, at, :] = turn(unit(yh, kgain).T, cos, sin).T.astype(BF16)
+        full = jnp.dot(value, wv[...], preferred_element_type=F32)
+        for h in range(2):
+            vt[h, :, at] = full[:, h * head_dim : (h + 1) * head_dim].T.astype(BF16)
+        send_kv(ph, start)
+        for h in range(4):
+            if h % 2 == 0:
+                full = jnp.dot(value, wq[:, h * head_dim : (h + 2) * head_dim], preferred_element_type=F32)
+            yh = full[:, (h % 2) * head_dim : (h % 2 + 1) * head_dim]
+            qt[h, :, at] = turn(unit(yh, qgain).T, cos, sin).astype(BF16)
+        send_q(ph, start)
+
+    def take_q(ph):
+        at = column((y + ph) % 2)
+        for j in range(1, 4):
+            m = (place + j) % 4
+            ref = qb.at[1, m, :, at]
+            remote(ref, ref, relay_send.at[0, 0], q_recv.at[1, m, ph], (s, partner)).wait_recv()
+            one = remote(ref, qb.at[0, m, :, at], relay_send.at[j, ph], q_recv.at[0, m, ph], (s, partner))
+            one.start()
+            sends.append(one)
+
+    for one in loads[2:]:
         one.wait()
-
-    def copy(i, src, h, way, peer):
-        b = bufs[i]
-        return remote(
-            b.at[src, h], b.at[src, h], send_sem.at[i, way], recv_sem.at[i, src], (peer, t)
+    remote(lat.at[partner], lat.at[partner], lat_send.at[0], lat_recv.at[2], (s, partner)).wait_recv()
+    project(0)
+    relay_rows(0)
+    cn = modulate(ctx[...], 1)
+    kc = jnp.dot(cn, wk[...], preferred_element_type=F32)
+    vc = jnp.dot(cn, wv[...], preferred_element_type=F32)
+    for h in range(2):
+        ckv[h, 0] = unit(kc[:, h * head_dim : (h + 1) * head_dim], kgain).astype(BF16)
+        ckv[h, 1] = vc[:, h * head_dim : (h + 1) * head_dim].astype(BF16)
+    send_ctx(start)
+    relay_rows(1)
+    take_q(0)
+    other = (1 - y) * 2 + 1 - c
+    for i, at in enumerate(pieces):
+        ref = lat.at[other, at]
+        remote(ref, ref, lat_send.at[0], lat_recv.at[3 + i], (s, partner)).wait_recv()
+    project(1)
+
+    local = owner & (target == c)
+
+    @pl.when(local)
+    def _():
+        kb[z] = kk[x]
+        vb[z] = vt[x]
+        cb[z] = ckv[x]
+
+    @pl.when(owner)
+    def _():
+        qb[1, place] = qt[x * 2 + c]
+        qb[0, place] = qt[x * 2 + 1 - c]
+
+    take_q(1)
+    for ph in range(2):
+        at = column((y + ph) % 2)
+        for j in range(4):
+            m = (place + j) % 4
+            for role in range(2) if j == 0 else range(1):
+                ref = qb.at[role, m, :, at]
+                one = remote(ref, ref, relay_send.at[0, 0], q_recv.at[role, m, ph], (s, partner))
+                if j == 0:
+                    pl.when(jnp.logical_not(owner))(one.wait_recv)
+                else:
+                    one.wait_recv()
+
+    def sweep(role, keys, values, bias, begin):
+        count = keys().shape[0]
+
+        def stage_a(m):
+            score[m % 2, :count] = jnp.dot(keys(), qb[role, m], preferred_element_type=F32)
+
+        def stage_b(m):
+            sc = score[m % 2, :count]
+            new = jnp.max(sc, axis=0, keepdims=True) + bias
+            if not begin:
+                old = top[role, m]
+                new = jnp.maximum(old, new)
+                f = jnp.exp2(old - new)
+                fade[m % 2] = f
+            p = jnp.exp2(sc - (new - bias))
+            line = jnp.sum(p, axis=0, keepdims=True)
+            ttl[role, m] = line if begin else ttl[role, m] * f + line
+            top[role, m] = new
+            prob[m % 2, :count] = p.astype(BF16)
+
+        def stage_c(m):
+            value = jnp.dot(values(), prob[m % 2, :count], preferred_element_type=F32)
+            acc[role, m] = value if begin else acc[role, m] * fade[m % 2] + value
+
+        for n in range(6):
+            if n < 4:
+                stage_a(n)
+            if 1 <= n <= 4:
+                stage_b(n - 1)
+            if n >= 2:
+                stage_c(n - 2)
+
+    for k in range(z_count):
+
+        @pl.when(jnp.logical_not(local & (k == z)))
+        def _():
+            remote(cb.at[k], cb.at[k], c_send.at[0, 0], c_recv.at[k], (s, partner)).wait_recv()
+
+    ctx_keys = jnp.concatenate([cb[k, 0] for k in range(z_count)], axis=0)
+    ctx_values = jnp.concatenate([cb[k, 1] for k in range(z_count)], axis=0)
+    ctx_values = ctx_values.astype(F32).T.astype(BF16)
+    for role in range(2):
+        sweep(role, lambda: ctx_keys, lambda: ctx_values, lift * math.log2(math.e), True)
+
+    give = [
+        remote(acc.at[0, m], acc_in.at[m], a_send.at[m], a_recv.at[m], (s, partner)) for m in range(4)
+    ]
+    give_stats = remote(stats, stats_in, s_sem.at[0], s_sem.at[1], (s, partner))
+
+    def step(n, carry):
+        k, role = n // 2, n % 2
+        zz = ((quad + k // 2) % quads) * 2 + (low + k % 2) % 2
+
+        @pl.when((role == 0) & jnp.logical_not(local & (zz == z)))
+        def _():
+            for ph in range(2):
+                at = column((y + ph) % 2)
+                for kind, ref in ((0, kb.at[zz, at]), (1, vb.at[zz, :, at])):
+                    remote(ref, ref, kv_send.at[0, 0, 0, 0], kv_recv.at[kind, ph, zz], (s, partner)).wait_recv()
+
+        sweep(role, lambda: kb[zz], lambda: vb[zz], 0.0, False)
+
+        @pl.when(n == 2 * z_count - 2)
+        def _():
+            for m in range(4):
+                stats[m, 0:1] = top[0, m]
+                stats[m, 1:2] = ttl[0, m]
+            for one in give + [give_stats]:
+                one.start()
+
+        return carry
+
+    lax.fori_loop(0, 2 * z_count, step, 0)
+    give_stats.wait_recv()
+    for one in give:
+        one.wait_recv()
+
+    def return_o(m, half, act):
+        to = (quad * 2 + m // 2) * 2 + m % 2
+        yy = (1 - y + half) % 2
+        at = column(yy)
+        head = pl.ds(pl.multiple_of((x * 2 + c) * head_dim, head_dim), head_dim)
+        here = (to == s) & owner
+
+        @pl.when(jnp.logical_not(here))
+        def _():
+            act(remote(
+                ob.at[m, at], att.at[at, head], o_send.at[m, half],
+                o_recv.at[x * 2 + c, half], (to, y * 2 + low),
+            ))
+
+        if act is start:
+
+            @pl.when(here)
+            def _():
+                att[at, head] = ob[m, at]
+
+    for half in range(2):
+        at = column((1 - y + half) % 2)
+        for j in range(4):
+            m = j
+            a, b = top[1, m, :, at], stats_in[m, 0:1, at]
+            peak = jnp.maximum(a, b)
+            wa, wb = jnp.exp2(a - peak), jnp.exp2(b - peak)
+            den = 1.0 / (ttl[1, m, :, at] * wa + stats_in[m, 1:2, at] * wb)
+            done = acc[1, m, :, at] * (wa * den) + acc_in[m, :, at] * (wb * den)
+            ob[m, at, :] = done.T.astype(BF16)
+            return_o(m, half, start)
+
+    step_cols = width // chunks
+
+    def piece(n, yy, cc):
+        at = pl.ds(pl.multiple_of((yy * 2 + cc) * rows, rows), rows)
+        return jnp.dot(
+            att[at, :], wo[:, n * step_cols : (n + 1) * step_cols], preferred_element_type=F32
         )
 
-    def source(k):
-        low = jnp.minimum(z, z_count - 1 - z)
-        both = k <= 2 * low
-        dist = jnp.where(both, (k + 1) // 2, k - low)
-        up = jnp.where(both, k % 2 == 1, z < z_count - 1 - z)
-        return jnp.where(up, z + dist, z - dist)
-
-    def line(act):
-        for dist in range(1, z_count):
-            for sign in (1, -1):
-                there = z + sign * dist
-
-                @pl.when((there >= 0) & (there < z_count))
-                def _():
-                    to = (there + z_count) % z_count
-                    for i in range(3):
-                        act(copy(i, s, to % 2, to, to * x_count + x))
-
-    def across(k, act):
-        zz = source(k)
-        src = zz * x_count + x
-        for i in range(3):
-            if act is None:
-
-                @pl.when(k > 0)
-                def _():
-                    copy(i, src, mine, 0, s).wait_recv()
-
-            for j in range(1, x_count):
-                way = z_count + zz * (x_count - 1) + j - 1
-                one = copy(i, src, mine, way, z * x_count + (x + j) % x_count)
-                one.start() if act is None else act(one)
-
-    def update(i, queries, keys, values_t, bias):
-        sc = jnp.dot(keys, queries, preferred_element_type=F32) * factor
-        if bias != 0.0:
-            sc = sc + bias
-        old = top[i]
-        new = jnp.maximum(old, jnp.max(sc, axis=0, keepdims=True))
-        p = jnp.exp2(sc - new)
-        f = jnp.exp2(old - new)
-        top[i] = new
-        tot[i] = tot[i] * f + jnp.sum(p, axis=0, keepdims=True)
-        acc[i] = acc[i] * f + jnp.dot(values_t, p.astype(BF16), preferred_element_type=F32)
-
-    def block(src):
-        def tile(i, carry):
-            update(i, qb[i // group, i % group], kb[src, mine], vb[src, mine], 0.0)
-            return carry
-
-        lax.fori_loop(0, 2 * group, tile, 0)
-
-    def step(k, carry):
-        across(k, None)
-
-        @pl.when(k == 0)
-        def _():
-            swap_q.wait_recv()
-
-        block(source(k) * x_count + x)
-
-        @pl.when(k > 0)
-        def _():
-            before = source(k - 1)
-            for j in range(1, x_count):
-                old = before * x_count + (x + j) % x_count
-                for i in range(3):
-                    copy(i, old, mine, 0, s).wait_recv()
-                block(old)
-
-        return carry
-
-    line(lambda one: one.start())
-    lax.fori_loop(0, z_count, step, 0)
-    final = source(z_count - 1)
-    ends = [final * x_count + (x + j) % x_count for j in range(1, x_count)]
-    for src in ends:
-        copy(0, src, mine, 0, s).wait_recv()
-    keys = jnp.concatenate([cb[j, mine, 0] for j in range(sp_count)], axis=0)
-    vals = jnp.concatenate([cb[j, mine, 1] for j in range(sp_count)], axis=0)
-    vals = vals.astype(F32).T.astype(BF16)
-    span = group * head_dim
-    swap_a = remote(ab.at[0], ab.at[1], swap_sem.at[2], swap_sem.at[3], (mate, t))
-    for who in range(2):
-        for g in range(group):
-            update(who * group + g, qb[who, g], keys, vals, lift * math.log2(math.e))
-        for src in ends:
-            if who == 0:
-                for i in (1, 2):
-                    copy(i, src, mine, 0, s).wait_recv()
-            for g in range(group):
-                update(who * group + g, qb[who, g], kb[src, mine], vb[src, mine], 0.0)
-        for g in range(group):
-            i = who * group + g
-            done = (acc[i] / tot[i]).T.astype(BF16)
-            if who == 0:
-                ab[0, :, g * head_dim : (g + 1) * head_dim] = done
+    units = [(half, n) for half in range(2) for n in range(chunks)]
+    cores = [
+        remote(core_out.at[h, n], core_in.at[h, n], core_send.at[h, n], core_recv.at[h, n], (s, partner))
+        for h, n in units
+    ]
+    mesh = [
+        remote(mesh_out.at[n], mesh_in.at[n], mesh_send.at[n], mesh_recv.at[n], (s, across))
+        for n in range(chunks)
+    ]
+    for u in range(len(units) + 1):
+        if u < len(units):
+            half, n = units[u]
+            yy = (1 - y + half) % 2
+            if n == 0:
+                for i in range(2):
+                    for g in range(2):
+                        ref = att.at[column(yy), pl.ds((i * 2 + g) * head_dim, head_dim)]
+                        one = remote(ref, ref, o_send.at[0, 0], o_recv.at[i * 2 + g, half], (s, partner))
+                        pl.when(jnp.logical_not(owner & (x == i) & (g == c)))(one.wait_recv)
+            core_out[half, n] = piece(n, yy, 1 - c).astype(BF16)
+            cores[u].start()
+        if u > 0:
+            half, n = units[u - 1]
+            value = piece(n, (1 - y + half) % 2, c)
+            cores[u - 1].wait_recv()
+            value = value + core_in[half, n].astype(F32)
+            if half == 0:
+                mesh_out[n] = value.astype(BF16)
+                mesh[n].start()
             else:
-                at = pl.ds(pl.multiple_of(mine * span + g * head_dim, head_dim), head_dim)
-                out_ref[:, at] = done
-        if who == 0:
-            swap_a.start()
-
-    def drain(k, carry):
-        across(k, lambda one: one.wait_send())
-        return carry
-
-    lax.fori_loop(0, z_count, drain, 0)
-    line(lambda one: one.wait_send())
-    swap_a.wait_recv()
-    out_ref[:, pl.ds(pl.multiple_of((1 - mine) * span, head_dim), span)] = ab[1]
-    swap_q.wait_send()
-    swap_a.wait_send()
+                mixed[n] = value
+    square = jnp.zeros((rows, 1), F32)
+    for n in range(chunks):
+        mesh[n].wait_recv()
+        value = mixed[n] + mesh_in[n].astype(F32)
+        mixed[n] = value
+        square = square + jnp.sum(value * value, axis=-1, keepdims=True)
+    inv = lax.rsqrt(square / width + NORM_EPS)
+    for n in range(chunks):
+        at = slice(n * step_cols, (n + 1) * step_cols)
+        gate = mod[0:1, 2 * width + n * step_cols : 2 * width + (n + 1) * step_cols]
+        out_ref[:, at] = (lat[t, :, at].astype(F32) + gate * (mixed[n] * inv)).astype(BF16)
+
+    def sent(one):
+        one.wait_send()
+
+    for one in sends + give + [give_stats] + cores + mesh:
+        one.wait_send()
+    for ph in range(2):
+        send_kv(ph, sent)
+        send_q(ph, sent)
+    send_ctx(sent)
+    for half in range(2):
+        for m in range(4):
+            return_o(m, half, sent)
 
 
 def mix_kernel(
@@ -549,7 +825,7 @@
         one.wait_send()
 
 
-def whole_kernel(sp_count, tp_count, x_count, head_dim, group, lift, chunks, paired, counts, *refs):
+def whole_kernel(sp_count, tp_count, x_count, head_dim, group, lift, chunks, counts, *refs):
     (
         cond, cond_1, mw, lat, ctx, wq, wk, wv, qg, kg, cos, sin, wo, lat_rows,
         out, qt, k, vt, ckv, gate, att, wo_vm, wo_sem, *rest,
@@ -560,8 +836,7 @@
         sp_count, tp_count, head_dim, cond, cond_1, mw, lat, ctx, wq, wk, wv, qg, kg, cos, sin,
         qt, k, vt, ckv, gate, *front_scratch, wo, wo_vm, wo_sem,
     )
-    attention = pair_kernel if paired else attend_kernel
-    attention(sp_count, x_count, group, lift, k, vt, ckv, qt, att, *middle_scratch)
+    attend_kernel(sp_count, x_count, group, lift, k, vt, ckv, qt, att, *middle_scratch)
     mix_kernel(
         tp_count, chunks, att, wo, wo_vm, wo_sem, lat_rows, gate, out, *rest[front + middle :]
     )
@@ -570,6 +845,104 @@
 ANY = pl.BlockSpec(memory_space=pl.ANY)
 VM = pl.BlockSpec(memory_space=pltpu.VMEM)
 DMA = pltpu.SemaphoreType.DMA
+
+
+def grid_tables(all_rows, head_dim):
+    quarter = head_dim // 4
+    lines = all_rows // GRID_W
+    row = lax.axis_index("sp") * lines + jnp.arange(lines, dtype=jnp.int32)
+    where = jnp.concatenate([row, jnp.arange(GRID_W, dtype=jnp.int32)]).astype(F32)
+    inv_freq = ROPE_BASE ** (-jnp.arange(quarter, dtype=F32) / quarter)
+    angles = inv_freq[:, None] * where[None, :]
+    small = lax.optimization_barrier((jnp.cos(angles), jnp.sin(angles)))
+    return [
+        jnp.stack([jnp.repeat(one[:, :lines], GRID_W, axis=1), jnp.tile(one[:, lines:], (1, lines))])
+        for one in small
+    ]
+
+
+def quad_call(args, out_weight, sp_count, head_dim, lift):
+    mod_weight, latents, context, query_weight, key_matrix, value_matrix = args[2:8]
+    rows, width = latents.shape
+    ctx_rows = context.shape[0]
+    mod_cols = mod_weight.shape[1]
+    all_rows, z_count, quads, chunks = 4 * rows, sp_count // 2, sp_count // 4, 4
+    step = width // chunks
+    cos, sin = grid_tables(all_rows, head_dim)
+    block = max(all_rows, z_count * ctx_rows)
+    scratch = [
+        pltpu.VMEM(mod_weight.shape, F32),
+        pltpu.VMEM((4, rows, width), BF16),
+        pltpu.VMEM(context.shape, BF16),
+        pltpu.VMEM(query_weight.shape, BF16),
+        pltpu.VMEM(key_matrix.shape, BF16),
+        pltpu.VMEM(value_matrix.shape, BF16),
+        pltpu.VMEM(out_weight.shape, BF16),
+        pltpu.VMEM(cos.shape, F32),
+        pltpu.VMEM(sin.shape, F32),
+        pltpu.VMEM((sp_count, 2, mod_cols), F32),
+        pltpu.VMEM((4, 2, mod_cols), F32),
+        pltpu.VMEM((2, 4 * mod_cols), F32),
+        pltpu.VMEM((2 * rows, width), BF16),
+        pltpu.VMEM((4, head_dim, all_rows), BF16),
+        pltpu.VMEM((2, all_rows, head_dim), BF16),
+        pltpu.VMEM((2, head_dim, all_rows), BF16),
+        pltpu.VMEM((2, 2, ctx_rows, head_dim), BF16),
+        pltpu.VMEM((2, 4, head_dim, all_rows), BF16),
+        pltpu.VMEM((z_count, all_rows, head_dim), BF16),
+        pltpu.VMEM((z_count, head_dim, all_rows), BF16),
+        pltpu.VMEM((z_count, 2, ctx_rows, head_dim), BF16),
+        pltpu.VMEM((2, 4, 1, all_rows), F32),
+        pltpu.VMEM((2, 4, 1, all_rows), F32),
+        pltpu.VMEM((2, 4, head_dim, all_rows), F32),
+        pltpu.VMEM((4, 2, all_rows), F32),
+        pltpu.VMEM((4, 2, all_rows), F32),
+        pltpu.VMEM((4, head_dim, all_rows), F32),
+        pltpu.VMEM((2, block, all_rows), F32),
+        pltpu.VMEM((2, block, all_rows), BF16),
+        pltpu.VMEM((2, 1, all_rows), F32),
+        pltpu.VMEM((4, all_rows, head_dim), BF16),
+        pltpu.VMEM((all_rows, 4 * head_dim), BF16),
+        pltpu.VMEM((2, chunks, rows, step), BF16),
+        pltpu.VMEM((2, chunks, rows, step), BF16),
+        pltpu.VMEM((chunks, rows, step), BF16),
+        pltpu.VMEM((chunks, rows, step), BF16),
+        pltpu.VMEM((chunks, rows, step), F32),
+        DMA((9,)),
+        DMA((5,)),
+        DMA((5,)),
+        DMA((sp_count,)),
+        DMA((sp_count,)),
+        DMA((4,)),
+        DMA((4,)),
+        DMA((2, 2, quads, 2)),
+        DMA((2, 2, z_count)),
+        DMA((quads, 2)),
+        DMA((z_count,)),
+        DMA((2, 2, 2)),
+        DMA((2, 4, 2)),
+        DMA((4, 2)),
+        DMA((4,)),
+        DMA((4,)),
+        DMA((2,)),
+        DMA((4, 2)),
+        DMA((4, 2)),
+        DMA((2, chunks)),
+        DMA((2, chunks)),
+        DMA((chunks,)),
+        DMA((chunks,)),
+    ]
+    return pl.pallas_call(
+        functools.partial(quad_kernel, sp_count, head_dim, lift, chunks),
+        out_shape=jax.ShapeDtypeStruct((rows, width), BF16),
+        in_specs=[VM, VM, ANY, ANY, ANY, ANY, ANY, ANY, VM, VM, ANY, ANY, ANY],
+        out_specs=VM,
+        scratch_shapes=scratch,
+        compiler_params=pltpu.CompilerParams(
+            collective_id=0, has_side_effects=True, vmem_limit_bytes=VMEM_BYTES
+        ),
+        name="quad",
+    )(*args, cos, sin, out_weight)
 
 
 def body(
@@ -594,15 +967,21 @@
     kv_heads = key_matrix.shape[1] // head_dim
     all_rows = rows * tp_count
     mod_cols = mod_weight.shape[1]
-    positions = lax.axis_index("sp") * all_rows + jnp.arange(all_rows, dtype=jnp.int32)
-    cos, sin = tables(positions, head_dim)
     lift = math.log(sp_count * all_rows / (2.0 * sp_count * ctx_rows))
     group = heads // kv_heads
-    paired = kv_heads == 2 and (sp_count // x_count) % 2 == 0
+    args = (
+        cond[None], ctx_cond[None], mod_weight, latents, context, query_weight, key_matrix, value_matrix,
+        query_gain[None], key_gain[None],
+    )
+    wide = all_rows % GRID_W == 0 and all_rows == rows * 4 and rows % 128 == 0
+    if wide and kv_heads == 2 and group == 2 and x_count == 2 and sp_count % 4 == 0:
+        return quad_call(args, out_weight, sp_count, head_dim, lift)
     chunks = 4
     y_count = tp_count // 2
     step = width // chunks
     far = max(y_count - 1, 1)
+    positions = lax.axis_index("sp") * all_rows + jnp.arange(all_rows, dtype=jnp.int32)
+    cos, sin = tables(positions, head_dim)
     shared = [
         pltpu.VMEM((heads, head_dim, all_rows), BF16),
         pltpu.VMEM((kv_heads, all_rows, head_dim), BF16),
@@ -640,16 +1019,7 @@
         pltpu.VMEM((heads, head_dim, all_rows), F32),
         DMA((3,)),
     ]
-    if paired:
-        middle += [
-            pltpu.VMEM((2, group, head_dim, all_rows), BF16),
-            pltpu.VMEM((2, all_rows, group * head_dim), BF16),
-            DMA((3, sp_count)),
-            DMA((3, sp_count)),
-            DMA((4,)),
-        ]
-    else:
-        middle += [DMA((3, sp_count, x_count + 1)), DMA((3, sp_count))]
+    middle += [DMA((3, sp_count, x_count + 1)), DMA((3, sp_count))]
     last = [
         pltpu.VMEM((chunks, y_count, rows, step), BF16),
         pltpu.VMEM((chunks, y_count, rows, step), BF16),
@@ -664,7 +1034,7 @@
     counts = (len(front), len(middle), len(last))
     return pl.pallas_call(
         functools.partial(
-            whole_kernel, sp_count, tp_count, x_count, head_dim, group, lift, chunks, paired, counts
+            whole_kernel, sp_count, tp_count, x_count, head_dim, group, lift, chunks, counts
         ),
         out_shape=jax.ShapeDtypeStruct((rows, width), BF16),
         in_specs=[VM, VM, ANY, ANY, VM, ANY, ANY, ANY, VM, VM, VM, VM, ANY, VM],
@@ -675,8 +1045,7 @@
         ),
         name="whole",
     )(
-        cond[None], ctx_cond[None], mod_weight, latents, context, query_weight, key_matrix, value_matrix,
-        query_gain[None], key_gain[None], cos, sin, out_weight, latents,
+        *args, cos, sin, out_weight, latents,
     )
 
 

time: 92.9 us -> 88 us (0.947)
  Pallas kernels: 88.5 us -> 84 us
    pallas_call x1, Pallas kernels: 88.5 us -> 84 us  [quad_call(): pl.pallas_call(functools.partial(quad_kernel, sp_count, head_dim, lift, c...]
    sin x1, other arithmetic: 1.23 us -> 0.14 us  [grid_tables(): small = lax.optimization_barrier((jnp.cos(angles), jnp.sin(angles)))]
where the time goes in v1:
time: 88 us; the launch traced here: 87.6 us
  Pallas kernels  84 us (95%)
  local copies, waits for them, and re-layouts  2.6 us (3%)
  other arithmetic  0.94 us (1%)
    pallas_call x1, Pallas kernels, quad_call(): pl.pallas_call(functools.partial(quad_kernel, sp_count, head_dim, lift, c...  84 us
    unnamed x1, local copies, waits for them, and re-layouts  1.88 us

profile of v1, /device:TPU:1, one launch (start us, length us, event | category | flops | bytes accessed | tf_op | source)
XLA Modules:
  0.0 87.6 jit_solution(7586464978326014984)
XLA Ops:
  0.0 0.1 add_convert_fusion
  0.1 0.1 multiply_sine_fusion
  0.2 0.1 slice.13
  0.3 0.1 slice.15
  0.4 0.1 tile.19
  0.5 0.1 tile.17
  0.6 0.1 broadcast_in_dim.25
  0.7 0.1 stack_reshape.7
  0.8 0.1 broadcast_in_dim.24
  0.9 0.1 stack_reshape.6
  1.0 0.7 pad_maximum_fusion
  1.7 84.0 %quad.1 = bf16[128,2048]{1,0:T(8,128)(2,1)} custom-call(f32[1,256]{1,0:T(1,128)} %bitcast.8, f32[1,256]{1,0:T(1,128)} %bitcast.9, f32[256,1536]{1,0:T(8,128)} %refs_2_.1, bf16[128,2048]{1,0:T(8,128)(2,1)} %refs_3_.1, bf16[64,2048]{1,0:T(8,128)(2,1)} %refs_4_.1, bf16[2048,512]{1,0:T(8,128)(2,1)} %refs_5_.1, bf16[2048,256]{1,0:T(8,128)(2,1)} %refs_6_.1, ...), custom_call_target="tpu_custom_call" | custom-call | tf_op jit(solution)/shard_map/quad/pallas_call | solution.py:935
  85.7 1.9 %copy.13 = bf16[128,2048]{1,0:T(8,128)(2,1)} copy(bf16[128,2048]{1,0:T(8,128)(2,1)} %quad.1) | data formatting | bytes 1048576
  (5 shorter events, 0.0 us)

commit v2 on v1

--- a/solution.py
+++ b/solution.py
@@ -3,6 +3,7 @@
 
 import jax
 import jax.numpy as jnp
+import numpy as np
 from jax import lax
 from jax.experimental import pallas as pl
 from jax.experimental.pallas import tpu as pltpu
@@ -328,15 +329,16 @@
 
 def quad_kernel(sp_count, head_dim, lift, chunks, *refs):
     (
-        cond_ref, cond_1_ref, mw_hbm, lat_hbm, ctx_hbm, wq_hbm, wk_hbm, wv_hbm, qg_ref, kg_ref,
+        cond_hbm, cond_1_hbm, mw_hbm, lat_hbm, ctx_hbm, wq_hbm, wk_hbm, wv_hbm, qg_hbm, kg_hbm,
         cos_hbm, sin_hbm, wo_hbm,
         out_ref,
+        cond_ref, cond_1_ref, qg_ref, kg_ref, cos_in, sin_in, small_sem,
         mw, lat, ctx, wq, wk, wv, wo, cos_ref, sin_ref, part, tot, mod, xn,
-        qt, kk, vt, ckv, qb, kb, vb, cb, top, ttl, acc, stats, stats_in, acc_in,
+        qt, kk, vt, ckv, qb, kb, vb, cb, stat, acc, stat_in, acc_in,
         score, prob, fade, ob, att, core_out, core_in, mesh_out, mesh_in, mixed,
         load_sem, lat_send, lat_recv, part_send, part_recv, tot_send, tot_recv,
-        kv_send, kv_recv, c_send, c_recv, q_send, q_recv, relay_send,
-        a_send, a_recv, s_sem, o_send, o_recv, core_send, core_recv, mesh_send, mesh_recv,
+        kv_send, kv_recv, c_send, c_recv, q_send, q_recv, relay_send, pass_send,
+        a_send, a_recv, s_send, s_recv, o_send, o_recv, core_send, core_recv, mesh_send, mesh_recv,
     ) = refs
     s, t = lax.axis_index("sp"), lax.axis_index("tp")
     y, c = t // 2, t % 2
@@ -351,14 +353,19 @@
     rows, width = lat.shape[1], lat.shape[2]
     all_rows = 4 * rows
     span = 2 * rows
-    first = max(rows * 3 // 128 * 16, 16)
+    first = rows // 64 * 16
 
     load_pairs = (
-        (lat_hbm, lat.at[t]), (mw_hbm, mw), (wk_hbm, wk), (wv_hbm, wv), (wq_hbm, wq), (ctx_hbm, ctx),
-        (cos_hbm, cos_ref), (sin_hbm, sin_ref), (wo_hbm, wo),
+        (mw_hbm, mw), (lat_hbm, lat.at[t]), (wk_hbm, wk), (wv_hbm, wv), (wq_hbm, wq), (ctx_hbm, ctx),
+        (wo_hbm, wo),
     )
     loads = [pltpu.make_async_copy(a, b, load_sem.at[i]) for i, (a, b) in enumerate(load_pairs)]
-    for one in loads:
+    small_pairs = (
+        (cond_hbm, cond_ref), (cond_1_hbm, cond_1_ref), (cos_hbm.at[s], cos_in), (sin_hbm.at[s], sin_in),
+        (qg_hbm, qg_ref), (kg_hbm, kg_ref),
+    )
+    smalls = [pltpu.make_async_copy(a, b, small_sem.at[i]) for i, (a, b) in enumerate(small_pairs)]
+    for one in loads[:1] + smalls + loads[1:2]:
         one.start()
 
     barrier = pltpu.get_barrier_semaphore()
@@ -371,14 +378,27 @@
         dev = (s, (1 - y) * 2 + (c + k) % 2)
         pl.semaphore_signal(barrier, inc=1, device_id=dev, device_id_type=MESH)
 
-    loads[1].wait()
+    for one in smalls:
+        one.wait()
+    for small, table in ((cos_in, cos_ref), (sin_in, sin_ref)):
+        for n in range(all_rows // 128):
+            at = slice(n * 128, (n + 1) * 128)
+            parts = [
+                jnp.broadcast_to(small[0, :, r : r + 1], (small.shape[1], GRID_W))
+                for r in range(n * 128 // GRID_W, (n + 1) * 128 // GRID_W)
+            ]
+            table[0, :, at] = jnp.concatenate(parts, axis=1)
+            table[1, :, at] = small[1]
+    loads[0].wait()
+    for one in loads[2:]:
+        one.start()
     lines = lax.broadcasted_iota(jnp.int32, (8, cond_ref.shape[1]), 0)
     cond = jnp.where(lines == 0, cond_ref[...], jnp.where(lines == 1, cond_1_ref[...], 0.0))
     cond = cond * jax.nn.sigmoid(cond)
     part[s] = jnp.dot(
         cond, mw[...], precision=lax.Precision.HIGHEST, preferred_element_type=F32
     )[:2]
-    loads[0].wait()
+    loads[1].wait()
     pl.semaphore_wait(barrier, 2 * sp_count + 1)
 
     sends = [
@@ -452,35 +472,78 @@
         here = (to == s) & (target == c)
         return to, here
 
-    def send_kv(ph, act):
-        at = column((y + ph) % 2)
+    def free(n):
+        return (low == 1) == ((quad + n) % quads > quad)
+
+    def row_spot(lo):
+        return pl.ds(pl.multiple_of(lo * span, span), span)
+
+    def allowed(n, which):
+        if n == 0:
+            return which in ("own", "all")
+        if which == "own":
+            return False
+        straight = {"early": free(n), "late": jnp.logical_not(free(n)) & (c == low)}
+        return straight[which] if which in straight else free(n) | (c == low)
+
+    def send_kv(ph, kinds, which, act):
+        at, spot = column((y + ph) % 2), row_spot(low)
         for n in range(quads):
+            ok = allowed(n, which)
+            if ok is False:
+                continue
             for i in range(2):
                 to, here = dest(i, n)
-                for kind, src, dst in (
-                    (0, kk.at[i, at], kb.at[z, at]), (1, vt.at[i, :, at], vb.at[z, :, at]),
-                ):
-
-                    @pl.when(jnp.logical_not(here))
+                for kind in kinds:
+                    src, dst = (
+                        (kk.at[i, at], kb.at[quad, ph, spot]),
+                        (vt.at[i, :, at], vb.at[quad, ph, :, spot]),
+                    )[kind]
+
+                    @pl.when(jnp.logical_not(here) & ok)
                     def _():
                         act(remote(
                             src, dst, kv_send.at[kind, ph, n, i], kv_recv.at[kind, ph, z],
                             (to, y * 2 + target),
                         ))
 
-    def send_ctx(act):
+    def send_ctx(which, act):
         for n in range(quads):
+            ok = allowed(n, which)
+            if ok is False:
+                continue
             for i in range(2):
                 to, here = dest(i, n)
 
-                @pl.when(jnp.logical_not(here))
+                @pl.when(jnp.logical_not(here) & ok)
                 def _():
                     act(remote(
                         ckv.at[i], cb.at[z], c_send.at[n, i], c_recv.at[z], (to, y * 2 + target)
                     ))
 
+    def pass_on(ph, act):
+        spot = row_spot(1 - low)
+        for n in range(1, quads):
+            to = (((quad + n) % quads) * 2 + low) * 2 + x
+            if ph is None:
+                copies = [remote(cb.at[mate], cb.at[mate], pass_send.at[4, n], c_recv.at[mate], (to, t))]
+            else:
+                copies = [
+                    remote(ref, ref, pass_send.at[2 * ph + kind, n], kv_recv.at[kind, ph, mate], (to, t))
+                    for kind, ref in ((0, kb.at[quad, ph, spot]), (1, vb.at[quad, ph, :, spot]))
+                ]
+
+            @pl.when(free(n))
+            def _():
+                for one in copies:
+                    act(one)
+
+    def spot_of(m):
+        return m // 2, pl.ds(pl.multiple_of(m % 2 * span, span), span)
+
     def send_q(ph, act):
         at = column((y + ph) % 2)
+        pair, lanes = spot_of(place)
         for i in range(2):
             to = (quad * 2 + c) * 2 + i
             for g in range(2):
@@ -490,15 +553,15 @@
                 @pl.when(mine)
                 def _():
                     act(remote(
-                        src, qb.at[0, place, :, at], q_send.at[ph, i, g], q_recv.at[0, place, ph],
-                        (s, partner),
+                        src, qb.at[0, ph, pair, :, lanes], q_send.at[ph, i, g],
+                        q_recv.at[0, place, ph], (s, partner),
                     ))
 
                 @pl.when(jnp.logical_not(mine))
                 def _():
                     act(remote(
-                        src, qb.at[1, place, :, at], q_send.at[ph, i, g], q_recv.at[1, place, ph],
-                        (to, y * 2 + g),
+                        src, qb.at[1, ph, pair, :, lanes], q_send.at[ph, i, g],
+                        q_recv.at[1, place, ph], (to, y * 2 + g),
                     ))
 
     def start(one):
@@ -511,31 +574,113 @@
         value = xn[...]
         at = column(yy)
         cos, sin = cos_ref[:, :, at], sin_ref[:, :, at]
-        full = jnp.dot(value, wk[...], preferred_element_type=F32)
-        for h in range(2):
-            yh = full[:, h * head_dim : (h + 1) * head_dim]
-            kk[h, at, :] = turn(unit(yh, kgain).T, cos, sin).T.astype(BF16)
-        full = jnp.dot(value, wv[...], preferred_element_type=F32)
-        for h in range(2):
-            vt[h, :, at] = full[:, h * head_dim : (h + 1) * head_dim].T.astype(BF16)
-        send_kv(ph, start)
-        for h in range(4):
-            if h % 2 == 0:
-                full = jnp.dot(value, wq[:, h * head_dim : (h + 2) * head_dim], preferred_element_type=F32)
-            yh = full[:, (h % 2) * head_dim : (h % 2 + 1) * head_dim]
-            qt[h, :, at] = turn(unit(yh, qgain).T, cos, sin).astype(BF16)
-        send_q(ph, start)
+        spot = row_spot(low)
+
+        def keys():
+            full = jnp.dot(value, wk[...], preferred_element_type=F32)
+            for h in range(2):
+                yh = full[:, h * head_dim : (h + 1) * head_dim]
+                kk[h, at, :] = turn(unit(yh, kgain).T, cos, sin).T.astype(BF16)
+            send_kv(ph, (0,), "early", start)
+            send_kv(ph, (0,), "own", start)
+
+        def values():
+            full = jnp.dot(value, wv[...], preferred_element_type=F32)
+            for h in range(2):
+                vt[h, :, at] = full[:, h * head_dim : (h + 1) * head_dim].T.astype(BF16)
+            send_kv(ph, (1,), "early", start)
+            send_kv(ph, (1,), "own", start)
+
+            @pl.when(local)
+            def _():
+                kb[quad, ph, spot] = kk[x, at]
+                vb[quad, ph, :, spot] = vt[x, :, at]
+
+        def queries():
+            for h in range(4):
+                if h % 2 == 0:
+                    full = jnp.dot(
+                        value, wq[:, h * head_dim : (h + 2) * head_dim], preferred_element_type=F32
+                    )
+                yh = full[:, (h % 2) * head_dim : (h % 2 + 1) * head_dim]
+                qt[h, :, at] = turn(unit(yh, qgain).T, cos, sin).astype(BF16)
+            send_q(ph, start)
+            pair, lanes = spot_of(place)
+
+            @pl.when(owner)
+            def _():
+                qb[1, ph, pair, :, lanes] = qt[x * 2 + c, :, at]
+                qb[0, ph, pair, :, lanes] = qt[x * 2 + 1 - c, :, at]
+
+        if ph == 1:
+            queries()
+            for which in ("early", "own", "late"):
+                send_ctx(which, start)
+        keys()
+        values()
+        if ph == 0:
+            queries()
+        send_kv(ph, (0, 1), "late", start)
 
     def take_q(ph):
-        at = column((y + ph) % 2)
         for j in range(1, 4):
             m = (place + j) % 4
-            ref = qb.at[1, m, :, at]
+            pair, lanes = spot_of(m)
+            ref = qb.at[1, ph, pair, :, lanes]
             remote(ref, ref, relay_send.at[0, 0], q_recv.at[1, m, ph], (s, partner)).wait_recv()
-            one = remote(ref, qb.at[0, m, :, at], relay_send.at[j, ph], q_recv.at[0, m, ph], (s, partner))
+            one = remote(
+                ref, qb.at[0, ph, pair, :, lanes], relay_send.at[j, ph], q_recv.at[0, m, ph],
+                (s, partner),
+            )
             one.start()
             sends.append(one)
 
+    def have_q(ph):
+        for j in range(4):
+            m = (place + j) % 4
+            pair, lanes = spot_of(m)
+            for role in range(2) if j == 0 else range(1):
+                ref = qb.at[role, ph, pair, :, lanes]
+                one = remote(ref, ref, relay_send.at[0, 0], q_recv.at[role, m, ph], (s, partner))
+                if j == 0:
+                    pl.when(jnp.logical_not(owner))(one.wait_recv)
+                else:
+                    one.wait_recv()
+
+    def wait_kv(zz, ph):
+        spot = row_spot(zz % 2)
+        for kind, ref in ((0, kb.at[zz // 2, ph, spot]), (1, vb.at[zz // 2, ph, :, spot])):
+            remote(ref, ref, kv_send.at[0, 0, 0, 0], kv_recv.at[kind, ph, zz], (s, partner)).wait_recv()
+
+    def have_kv(goal, ph):
+        for lo in range(2):
+            wait_kv(goal * 2 + lo, ph)
+
+    mate = quad * 2 + 1 - low
+    inner = functools.reduce(jnp.logical_or, [free(n) for n in range(1, quads)], low < 0)
+
+    def take_mate(ph):
+        @pl.when(inner)
+        def _():
+            wait_kv(mate, ph)
+
+        pass_on(ph, start)
+
+    def have_own(ph):
+        @pl.when(jnp.logical_not(inner))
+        def _():
+            wait_kv(mate, ph)
+
+        @pl.when(jnp.logical_not(local))
+        def _():
+            wait_kv(z, ph)
+
+    local = owner & (target == c)
+    stat[...] = jnp.concatenate(
+        [jnp.full(stat.shape[:3] + (1, all_rows), -1e30, F32), jnp.zeros(stat.shape[:3] + (1, all_rows), F32)],
+        axis=3,
+    )
+    acc[...] = jnp.zeros_like(acc)
     for one in loads[2:]:
         one.wait()
     remote(lat.at[partner], lat.at[partner], lat_send.at[0], lat_recv.at[2], (s, partner)).wait_recv()
@@ -547,64 +692,41 @@
     for h in range(2):
         ckv[h, 0] = unit(kc[:, h * head_dim : (h + 1) * head_dim], kgain).astype(BF16)
         ckv[h, 1] = vc[:, h * head_dim : (h + 1) * head_dim].astype(BF16)
-    send_ctx(start)
+
+    @pl.when(local)
+    def _():
+        cb[z] = ckv[x]
+
     relay_rows(1)
-    take_q(0)
+    take_mate(0)
     other = (1 - y) * 2 + 1 - c
     for i, at in enumerate(pieces):
         ref = lat.at[other, at]
         remote(ref, ref, lat_send.at[0], lat_recv.at[3 + i], (s, partner)).wait_recv()
     project(1)
 
-    local = owner & (target == c)
-
-    @pl.when(local)
-    def _():
-        kb[z] = kk[x]
-        vb[z] = vt[x]
-        cb[z] = ckv[x]
-
-    @pl.when(owner)
-    def _():
-        qb[1, place] = qt[x * 2 + c]
-        qb[0, place] = qt[x * 2 + 1 - c]
-
-    take_q(1)
-    for ph in range(2):
-        at = column((y + ph) % 2)
-        for j in range(4):
-            m = (place + j) % 4
-            for role in range(2) if j == 0 else range(1):
-                ref = qb.at[role, m, :, at]
-                one = remote(ref, ref, relay_send.at[0, 0], q_recv.at[role, m, ph], (s, partner))
-                if j == 0:
-                    pl.when(jnp.logical_not(owner))(one.wait_recv)
-                else:
-                    one.wait_recv()
-
-    def sweep(role, keys, values, bias, begin):
+    def sweep(ph, keys, values, bias):
         count = keys().shape[0]
 
-        def stage_a(m):
-            score[m % 2, :count] = jnp.dot(keys(), qb[role, m], preferred_element_type=F32)
-
-        def stage_b(m):
-            sc = score[m % 2, :count]
-            new = jnp.max(sc, axis=0, keepdims=True) + bias
-            if not begin:
-                old = top[role, m]
-                new = jnp.maximum(old, new)
-                f = jnp.exp2(old - new)
-                fade[m % 2] = f
+        def stage_a(n):
+            score[n % 2, :count] = jnp.dot(keys(), qb[n // 2, ph, n % 2], preferred_element_type=F32)
+
+        def stage_b(n):
+            sc = score[n % 2, :count]
+            old = stat[ph, n // 2, n % 2, 0:1]
+            new = jnp.maximum(old, jnp.max(sc, axis=0, keepdims=True) + bias)
+            f = jnp.exp2(old - new)
+            fade[n % 2] = f
             p = jnp.exp2(sc - (new - bias))
-            line = jnp.sum(p, axis=0, keepdims=True)
-            ttl[role, m] = line if begin else ttl[role, m] * f + line
-            top[role, m] = new
-            prob[m % 2, :count] = p.astype(BF16)
-
-        def stage_c(m):
-            value = jnp.dot(values(), prob[m % 2, :count], preferred_element_type=F32)
-            acc[role, m] = value if begin else acc[role, m] * fade[m % 2] + value
+            stat[ph, n // 2, n % 2, 1:2] = (
+                stat[ph, n // 2, n % 2, 1:2] * f + jnp.sum(p, axis=0, keepdims=True)
+            )
+            stat[ph, n // 2, n % 2, 0:1] = new
+            prob[n % 2, :count] = p.astype(BF16)
+
+        def stage_c(n):
+            value = jnp.dot(values(), prob[n % 2, :count], preferred_element_type=F32)
+            acc[ph, n // 2, n % 2] = acc[ph, n // 2, n % 2] * fade[n % 2] + value
 
         for n in range(6):
             if n < 4:
@@ -614,82 +736,73 @@
             if n >= 2:
                 stage_c(n - 2)
 
-    for k in range(z_count):
-
-        @pl.when(jnp.logical_not(local & (k == z)))
-        def _():
-            remote(cb.at[k], cb.at[k], c_send.at[0, 0], c_recv.at[k], (s, partner)).wait_recv()
-
-    ctx_keys = jnp.concatenate([cb[k, 0] for k in range(z_count)], axis=0)
-    ctx_values = jnp.concatenate([cb[k, 1] for k in range(z_count)], axis=0)
-    ctx_values = ctx_values.astype(F32).T.astype(BF16)
-    for role in range(2):
-        sweep(role, lambda: ctx_keys, lambda: ctx_values, lift * math.log2(math.e), True)
-
-    give = [
-        remote(acc.at[0, m], acc_in.at[m], a_send.at[m], a_recv.at[m], (s, partner)) for m in range(4)
-    ]
-    give_stats = remote(stats, stats_in, s_sem.at[0], s_sem.at[1], (s, partner))
-
-    def step(n, carry):
-        k, role = n // 2, n % 2
-        zz = ((quad + k // 2) % quads) * 2 + (low + k % 2) % 2
-
-        @pl.when((role == 0) & jnp.logical_not(local & (zz == z)))
-        def _():
-            for ph in range(2):
-                at = column((y + ph) % 2)
-                for kind, ref in ((0, kb.at[zz, at]), (1, vb.at[zz, :, at])):
-                    remote(ref, ref, kv_send.at[0, 0, 0, 0], kv_recv.at[kind, ph, zz], (s, partner)).wait_recv()
-
-        sweep(role, lambda: kb[zz], lambda: vb[zz], 0.0, False)
-
-        @pl.when(n == 2 * z_count - 2)
-        def _():
-            for m in range(4):
-                stats[m, 0:1] = top[0, m]
-                stats[m, 1:2] = ttl[0, m]
-            for one in give + [give_stats]:
-                one.start()
-
-        return carry
-
-    lax.fori_loop(0, 2 * z_count, step, 0)
-    give_stats.wait_recv()
-    for one in give:
-        one.wait_recv()
-
-    def return_o(m, half, act):
+    def give(ph):
+        return [
+            remote(acc.at[ph, 0], acc_in.at[ph], a_send.at[ph], a_recv.at[ph], (s, partner)),
+            remote(stat.at[ph, 0], stat_in.at[ph], s_send.at[ph], s_recv.at[ph], (s, partner)),
+        ]
+
+    def have_ctx(goal):
+        for lo in range(2):
+            k = goal * 2 + lo
+
+            @pl.when(jnp.logical_not(local & (k == z)))
+            def _():
+                remote(cb.at[k], cb.at[k], c_send.at[0, 0], c_recv.at[k], (s, partner)).wait_recv()
+
+    def sweeps(ph, late, begin, end, wait):
+        def one(j, carry):
+            goal = (quad + j) % quads
+            if wait:
+
+                @pl.when(j > 0)
+                def _():
+                    have_kv(goal, late)
+
+            sweep(ph, lambda: kb[goal, late], lambda: vb[goal, late], 0.0)
+            return carry
+
+        if end - begin == 1:
+            one(begin, 0)
+        elif end > begin:
+            lax.fori_loop(begin, end, one, 0)
+
+    def return_o(m, ph, cc, act):
         to = (quad * 2 + m // 2) * 2 + m % 2
-        yy = (1 - y + half) % 2
-        at = column(yy)
+        at = pl.ds(pl.multiple_of(((y + ph) % 2 * 2 + cc) * rows, rows), rows)
+        mine = pl.ds(cc * rows, rows)
         head = pl.ds(pl.multiple_of((x * 2 + c) * head_dim, head_dim), head_dim)
         here = (to == s) & owner
 
         @pl.when(jnp.logical_not(here))
         def _():
             act(remote(
-                ob.at[m, at], att.at[at, head], o_send.at[m, half],
-                o_recv.at[x * 2 + c, half], (to, y * 2 + low),
+                ob.at[m, ph, mine], att.at[at, head], o_send.at[m, ph, cc],
+                o_recv.at[x * 2 + c, ph, cc], (to, y * 2 + low),
             ))
 
         if act is start:
 
             @pl.when(here)
             def _():
-                att[at, head] = ob[m, at]
-
-    for half in range(2):
-        at = column((1 - y + half) % 2)
-        for j in range(4):
-            m = j
-            a, b = top[1, m, :, at], stats_in[m, 0:1, at]
-            peak = jnp.maximum(a, b)
-            wa, wb = jnp.exp2(a - peak), jnp.exp2(b - peak)
-            den = 1.0 / (ttl[1, m, :, at] * wa + stats_in[m, 1:2, at] * wb)
-            done = acc[1, m, :, at] * (wa * den) + acc_in[m, :, at] * (wb * den)
-            ob[m, at, :] = done.T.astype(BF16)
-            return_o(m, half, start)
+                att[at, head] = ob[m, ph, mine]
+
+    def merge(ph):
+        for one in give(ph):
+            one.wait_recv()
+        for cc in range(2):
+            for j in range(4):
+                m = (place + 3 - j) % 4
+                pair, half = m // 2, m % 2
+                lanes = pl.ds(pl.multiple_of(half * span + cc * rows, rows), rows)
+                a, b = stat[ph, 1, pair, 0:1, lanes], stat_in[ph, pair, 0:1, lanes]
+                peak = jnp.maximum(a, b)
+                wa, wb = jnp.exp2(a - peak), jnp.exp2(b - peak)
+                den = 1.0 / (stat[ph, 1, pair, 1:2, lanes] * wa + stat_in[ph, pair, 1:2, lanes] * wb)
+                done = acc[ph, 1, pair, :, lanes] * (wa * den) + acc_in[ph, pair, :, lanes] * (wb * den)
+                ob[m, ph, cc * rows : (cc + 1) * rows] = done.T.astype(BF16)
+            for j in range(4):
+                return_o((place + 3 - j) % 4, ph, cc, start)
 
     step_cols = width // chunks
 
@@ -699,37 +812,97 @@
             att[at, :], wo[:, n * step_cols : (n + 1) * step_cols], preferred_element_type=F32
         )
 
-    units = [(half, n) for half in range(2) for n in range(chunks)]
     cores = [
-        remote(core_out.at[h, n], core_in.at[h, n], core_send.at[h, n], core_recv.at[h, n], (s, partner))
-        for h, n in units
+        [
+            remote(core_out.at[h, n], core_in.at[h, n], core_send.at[h, n], core_recv.at[h, n], (s, partner))
+            for n in range(chunks)
+        ]
+        for h in range(2)
     ]
     mesh = [
         remote(mesh_out.at[n], mesh_in.at[n], mesh_send.at[n], mesh_recv.at[n], (s, across))
         for n in range(chunks)
     ]
-    for u in range(len(units) + 1):
-        if u < len(units):
-            half, n = units[u]
-            yy = (1 - y + half) % 2
-            if n == 0:
-                for i in range(2):
-                    for g in range(2):
-                        ref = att.at[column(yy), pl.ds((i * 2 + g) * head_dim, head_dim)]
-                        one = remote(ref, ref, o_send.at[0, 0], o_recv.at[i * 2 + g, half], (s, partner))
-                        pl.when(jnp.logical_not(owner & (x == i) & (g == c)))(one.wait_recv)
-            core_out[half, n] = piece(n, yy, 1 - c).astype(BF16)
-            cores[u].start()
-        if u > 0:
-            half, n = units[u - 1]
-            value = piece(n, (1 - y + half) % 2, c)
-            cores[u - 1].wait_recv()
-            value = value + core_in[half, n].astype(F32)
-            if half == 0:
+
+    def have_o(ph, cc):
+        at = pl.ds(pl.multiple_of(((y + ph) % 2 * 2 + cc) * rows, rows), rows)
+        for i in range(2):
+            for g in range(2):
+                ref = att.at[at, pl.ds((i * 2 + g) * head_dim, head_dim)]
+                one = remote(ref, ref, o_send.at[0, 0, 0], o_recv.at[i * 2 + g, ph, cc], (s, partner))
+                pl.when(jnp.logical_not(owner & (x == i) & (g == c)))(one.wait_recv)
+
+    def mix(ph):
+        yy = (y + ph) % 2
+
+        def give_core(cc, n):
+            core_out[ph, n] = piece(n, yy, cc).astype(BF16)
+            cores[ph][n].start()
+
+        def take_core(n, value):
+            cores[ph][n].wait_recv()
+            value = value + core_in[ph, n].astype(F32)
+            if ph == 1:
                 mesh_out[n] = value.astype(BF16)
                 mesh[n].start()
             else:
                 mixed[n] = value
+
+        have_o(ph, 0)
+
+        @pl.when(c == 1)
+        def _():
+            for n in range(chunks):
+                give_core(0, n)
+            have_o(ph, 1)
+            for n in range(chunks):
+                take_core(n, piece(n, yy, 1))
+
+        @pl.when(c == 0)
+        def _():
+            for n in range(chunks):
+                mixed[n] = piece(n, yy, 0)
+            have_o(ph, 1)
+            for n in range(chunks):
+                give_core(1, n)
+                take_core(n, mixed[n])
+
+    take_q(0)
+    have_q(0)
+    have_own(0)
+    sweeps(0, 0, 0, 1, False)
+    sweeps(0, 0, 1, quads, True)
+    take_q(1)
+    have_q(1)
+    sweeps(1, 0, 0, 1, False)
+    have_ctx(quad)
+    pass_on(None, start)
+    take_mate(1)
+    sweeps(1, 0, 1, quads, False)
+    have_own(1)
+    sweeps(1, 1, 0, 1, False)
+    for n in range(1, quads):
+        have_ctx((quad + n) % quads)
+    ctx_keys = jnp.concatenate([cb[k, 0] for k in range(z_count)], axis=0)
+    ctx_values = jnp.concatenate([cb[k, 1] for k in range(z_count)], axis=0)
+    ctx_values = ctx_values.astype(F32).T.astype(BF16)
+
+    def sweep_ctx(ph):
+        sweep(ph, lambda: ctx_keys, lambda: ctx_values, lift * math.log2(math.e))
+
+    sweep_ctx(1)
+    sweeps(1, 1, 1, quads, True)
+    for one in give(1):
+        one.start()
+    sweeps(0, 1, 0, 1, False)
+    merge(1)
+    sweeps(0, 1, 1, quads, False)
+    sweep_ctx(0)
+    for one in give(0):
+        one.start()
+    mix(1)
+    merge(0)
+    mix(0)
     square = jnp.zeros((rows, 1), F32)
     for n in range(chunks):
         mesh[n].wait_recv()
@@ -745,15 +918,17 @@
     def sent(one):
         one.wait_send()
 
-    for one in sends + give + [give_stats] + cores + mesh:
+    for one in sends + give(0) + give(1) + cores[0] + cores[1] + mesh:
         one.wait_send()
     for ph in range(2):
-        send_kv(ph, sent)
+        send_kv(ph, (0, 1), "all", sent)
+        pass_on(ph, sent)
         send_q(ph, sent)
-    send_ctx(sent)
-    for half in range(2):
         for m in range(4):
-            return_o(m, half, sent)
+            for cc in range(2):
+                return_o(m, ph, cc, sent)
+    send_ctx("all", sent)
+    pass_on(None, sent)
 
 
 def mix_kernel(
@@ -847,18 +1022,13 @@
 DMA = pltpu.SemaphoreType.DMA
 
 
-def grid_tables(all_rows, head_dim):
-    quarter = head_dim // 4
-    lines = all_rows // GRID_W
-    row = lax.axis_index("sp") * lines + jnp.arange(lines, dtype=jnp.int32)
-    where = jnp.concatenate([row, jnp.arange(GRID_W, dtype=jnp.int32)]).astype(F32)
-    inv_freq = ROPE_BASE ** (-jnp.arange(quarter, dtype=F32) / quarter)
-    angles = inv_freq[:, None] * where[None, :]
-    small = lax.optimization_barrier((jnp.cos(angles), jnp.sin(angles)))
-    return [
-        jnp.stack([jnp.repeat(one[:, :lines], GRID_W, axis=1), jnp.tile(one[:, lines:], (1, lines))])
-        for one in small
-    ]
+def grid_tables(sp_count, all_rows, head_dim):
+    quarter, lines, lane = head_dim // 4, all_rows // GRID_W, np.arange(128)
+    inv_freq = np.float32(ROPE_BASE) ** (-np.arange(quarter, dtype=np.float32) / quarter)
+    rows = np.arange(sp_count)[:, None] * lines + lane[None, :] % lines
+    both = np.stack([rows, np.broadcast_to(lane % GRID_W, rows.shape)], axis=1).astype(np.float32)
+    angles = (both[:, :, None, :] * inv_freq[None, None, :, None]).astype(np.float32)
+    return jnp.asarray(np.cos(angles)), jnp.asarray(np.sin(angles))
 
 
 def quad_call(args, out_weight, sp_count, head_dim, lift):
@@ -868,9 +1038,16 @@
     mod_cols = mod_weight.shape[1]
     all_rows, z_count, quads, chunks = 4 * rows, sp_count // 2, sp_count // 4, 4
     step = width // chunks
-    cos, sin = grid_tables(all_rows, head_dim)
+    cos, sin = grid_tables(sp_count, all_rows, head_dim)
     block = max(all_rows, z_count * ctx_rows)
     scratch = [
+        pltpu.VMEM(args[0].shape, F32),
+        pltpu.VMEM(args[1].shape, F32),
+        pltpu.VMEM(args[8].shape, F32),
+        pltpu.VMEM(args[9].shape, F32),
+        pltpu.VMEM(cos.shape[1:], F32),
+        pltpu.VMEM(sin.shape[1:], F32),
+        DMA((6,)),
         pltpu.VMEM(mod_weight.shape, F32),
         pltpu.VMEM((4, rows, width), BF16),
         pltpu.VMEM(context.shape, BF16),
@@ -878,8 +1055,8 @@
         pltpu.VMEM(key_matrix.shape, BF16),
         pltpu.VMEM(value_matrix.shape, BF16),
         pltpu.VMEM(out_weight.shape, BF16),
-        pltpu.VMEM(cos.shape, F32),
-        pltpu.VMEM(sin.shape, F32),
+        pltpu.VMEM((2, head_dim // 4, all_rows), F32),
+        pltpu.VMEM((2, head_dim // 4, all_rows), F32),
         pltpu.VMEM((sp_count, 2, mod_cols), F32),
         pltpu.VMEM((4, 2, mod_cols), F32),
         pltpu.VMEM((2, 4 * mod_cols), F32),
@@ -888,27 +1065,25 @@
         pltpu.VMEM((2, all_rows, head_dim), BF16),
         pltpu.VMEM((2, head_dim, all_rows), BF16),
         pltpu.VMEM((2, 2, ctx_rows, head_dim), BF16),
-        pltpu.VMEM((2, 4, head_dim, all_rows), BF16),
-        pltpu.VMEM((z_count, all_rows, head_dim), BF16),
-        pltpu.VMEM((z_count, head_dim, all_rows), BF16),
+        pltpu.VMEM((2, 2, 2, head_dim, all_rows), BF16),
+        pltpu.VMEM((quads, 2, all_rows, head_dim), BF16),
+        pltpu.VMEM((quads, 2, head_dim, all_rows), BF16),
         pltpu.VMEM((z_count, 2, ctx_rows, head_dim), BF16),
-        pltpu.VMEM((2, 4, 1, all_rows), F32),
-        pltpu.VMEM((2, 4, 1, all_rows), F32),
-        pltpu.VMEM((2, 4, head_dim, all_rows), F32),
-        pltpu.VMEM((4, 2, all_rows), F32),
-        pltpu.VMEM((4, 2, all_rows), F32),
-        pltpu.VMEM((4, head_dim, all_rows), F32),
+        pltpu.VMEM((2, 2, 2, 2, all_rows), F32),
+        pltpu.VMEM((2, 2, 2, head_dim, all_rows), F32),
+        pltpu.VMEM((2, 2, 2, all_rows), F32),
+        pltpu.VMEM((2, 2, head_dim, all_rows), F32),
         pltpu.VMEM((2, block, all_rows), F32),
         pltpu.VMEM((2, block, all_rows), BF16),
         pltpu.VMEM((2, 1, all_rows), F32),
-        pltpu.VMEM((4, all_rows, head_dim), BF16),
+        pltpu.VMEM((4, 2, 2 * rows, head_dim), BF16),
         pltpu.VMEM((all_rows, 4 * head_dim), BF16),
         pltpu.VMEM((2, chunks, rows, step), BF16),
         pltpu.VMEM((2, chunks, rows, step), BF16),
         pltpu.VMEM((chunks, rows, step), BF16),
         pltpu.VMEM((chunks, rows, step), BF16),
         pltpu.VMEM((chunks, rows, step), F32),
-        DMA((9,)),
+        DMA((7,)),
         DMA((5,)),
         DMA((5,)),
         DMA((sp_count,)),
@@ -922,27 +1097,30 @@
         DMA((2, 2, 2)),
         DMA((2, 4, 2)),
         DMA((4, 2)),
-        DMA((4,)),
-        DMA((4,)),
+        DMA((5, quads)),
         DMA((2,)),
-        DMA((4, 2)),
-        DMA((4, 2)),
+        DMA((2,)),
+        DMA((2,)),
+        DMA((2,)),
+        DMA((4, 2, 2)),
+        DMA((4, 2, 2)),
         DMA((2, chunks)),
         DMA((2, chunks)),
         DMA((chunks,)),
         DMA((chunks,)),
     ]
-    return pl.pallas_call(
+    out = pl.pallas_call(
         functools.partial(quad_kernel, sp_count, head_dim, lift, chunks),
-        out_shape=jax.ShapeDtypeStruct((rows, width), BF16),
-        in_specs=[VM, VM, ANY, ANY, ANY, ANY, ANY, ANY, VM, VM, ANY, ANY, ANY],
+        out_shape=pltpu.VMEM((rows, width), BF16),
+        in_specs=[pl.BlockSpec(memory_space=pltpu.HBM)] * 13,
         out_specs=VM,
         scratch_shapes=scratch,
         compiler_params=pltpu.CompilerParams(
-            collective_id=0, has_side_effects=True, vmem_limit_bytes=VMEM_BYTES
+            collective_id=0, has_side_effects=True, vmem_limit_bytes=VMEM_BYTES - 2 * rows * width * 2
         ),
         name="quad",
     )(*args, cos, sin, out_weight)
+    return out
 
 
 def body(

time: 88 us -> 66.4 us (0.75)
  Pallas kernels: 84 us -> 65.4 us
  local copies, waits for them, and re-layouts: 2.6 us -> 0.8 us
  other arithmetic: 0.94 us -> 0 us
    pallas_call x1, Pallas kernels: 84 us -> 65.4 us  [quad_call(): pl.pallas_call(functools.partial(quad_kernel, sp_count, head_dim, lift, c...]
    unnamed x1, local copies, waits for them, and re-layouts: 1.88 us -> 0.8 us
where the time goes in v2:
time: 66.4 us; the launch traced here: 66.2 us
  Pallas kernels  65.4 us (98%)
  local copies, waits for them, and re-layouts  0.8 us (1%)
    pallas_call x1, Pallas kernels, quad_call(): pl.pallas_call(functools.partial(quad_kernel, sp_count, head_dim, lift, c...  65.4 us

profile of v2, /device:TPU:1, one launch (start us, length us, event | category | flops | bytes accessed | tf_op | source)
XLA Modules:
  0.0 66.2 jit_solution(5276218561166559725)
XLA Ops:
  0.0 65.4 %quad.1 = bf16[128,2048]{1,0:T(8,128)(2,1)S(1)} custom-call(f32[1,256]{1,0:T(1,128)} %bitcast.4, f32[1,256]{1,0:T(1,128)} %bitcast.5, f32[256,1536]{1,0:T(8,128)} %refs_2_.1, bf16[128,2048]{1,0:T(8,128)(2,1)} %refs_3_.1, bf16[64,2048]{1,0:T(8,128)(2,1)} %refs_4_.1, bf16[2048,512]{1,0:T(8,128)(2,1)} %refs_5_.1, bf16[2048,256]{1,0:T(8,128)(2,1)} %refs_6_.1, ...), custom_call_target="tpu_custom_call" | custom-call | tf_op jit(solution)/shard_map/quad/pallas_call | solution.py:1112
  65.4 0.8 %copy.15 = bf16[128,2048]{1,0:T(8,128)(2,1)} copy(bf16[128,2048]{1,0:T(8,128)(2,1)S(1)} %quad.1) | data formatting | bytes 1048576

commit v3 on v2

--- a/solution.py
+++ b/solution.py
@@ -333,12 +333,12 @@
         cos_hbm, sin_hbm, wo_hbm,
         out_ref,
         cond_ref, cond_1_ref, qg_ref, kg_ref, cos_in, sin_in, small_sem,
-        mw, lat, ctx, wq, wk, wv, wo, cos_ref, sin_ref, part, tot, mod, xn,
+        mw, lat, ctx, wq, wk, wv, wo, cos_ref, sin_ref, part, tot, mod, xn, xs,
         qt, kk, vt, ckv, qb, kb, vb, cb, stat, acc, stat_in, acc_in,
         score, prob, fade, ob, att, core_out, core_in, mesh_out, mesh_in, mixed,
         load_sem, lat_send, lat_recv, part_send, part_recv, tot_send, tot_recv,
-        kv_send, kv_recv, c_send, c_recv, q_send, q_recv, relay_send, pass_send,
-        a_send, a_recv, s_send, s_recv, o_send, o_recv, core_send, core_recv, mesh_send, mesh_recv,
+        kv_send, kv_recv, c_send, c_recv, q_send, q_recv, relay_send, pass_send, raw_send, raw_recv,
+        a_send, a_recv, s_send, s_recv, o_recv, core_recv, mesh_send, mesh_recv,
     ) = refs
     s, t = lax.axis_index("sp"), lax.axis_index("tp")
     y, c = t // 2, t % 2
@@ -353,10 +353,10 @@
     rows, width = lat.shape[1], lat.shape[2]
     all_rows = 4 * rows
     span = 2 * rows
-    first = rows // 64 * 16
+    cuts = (0, rows * 3 // 8 // 16 * 16, rows * 3 // 4 // 16 * 16, rows)
 
     load_pairs = (
-        (mw_hbm, mw), (lat_hbm, lat.at[t]), (wk_hbm, wk), (wv_hbm, wv), (wq_hbm, wq), (ctx_hbm, ctx),
+        (mw_hbm, mw), (lat_hbm, lat.at[t]), (wk_hbm, wk), (wv_hbm, wv), (wq_hbm, wq), (ctx_hbm, ctx.at[quad]),
         (wo_hbm, wo),
     )
     loads = [pltpu.make_async_copy(a, b, load_sem.at[i]) for i, (a, b) in enumerate(load_pairs)]
@@ -365,7 +365,7 @@
         (qg_hbm, qg_ref), (kg_hbm, kg_ref),
     )
     smalls = [pltpu.make_async_copy(a, b, small_sem.at[i]) for i, (a, b) in enumerate(small_pairs)]
-    for one in loads[:1] + smalls + loads[1:2]:
+    for one in smalls[:2] + loads[:1] + smalls[2:] + loads[1:2]:
         one.start()
 
     barrier = pltpu.get_barrier_semaphore()
@@ -380,6 +380,9 @@
 
     for one in smalls:
         one.wait()
+    lines = lax.broadcasted_iota(jnp.int32, (8, cond_ref.shape[1]), 0)
+    cond = jnp.where(lines == 0, cond_ref[...], jnp.where(lines == 1, cond_1_ref[...], 0.0))
+    cond = (cond * jax.nn.sigmoid(cond)).T
     for small, table in ((cos_in, cos_ref), (sin_in, sin_ref)):
         for n in range(all_rows // 128):
             at = slice(n * 128, (n + 1) * 128)
@@ -392,12 +395,8 @@
     loads[0].wait()
     for one in loads[2:]:
         one.start()
-    lines = lax.broadcasted_iota(jnp.int32, (8, cond_ref.shape[1]), 0)
-    cond = jnp.where(lines == 0, cond_ref[...], jnp.where(lines == 1, cond_1_ref[...], 0.0))
-    cond = cond * jax.nn.sigmoid(cond)
-    part[s] = jnp.dot(
-        cond, mw[...], precision=lax.Precision.HIGHEST, preferred_element_type=F32
-    )[:2]
+    for r in range(2):
+        part[s, r : r + 1, :] = jnp.sum(mw[...] * cond[:, r : r + 1], axis=0, keepdims=True)
     loads[1].wait()
     pl.semaphore_wait(barrier, 2 * sp_count + 1)
 
@@ -405,14 +404,21 @@
         remote(part.at[s], part.at[s], part_send.at[j], part_recv.at[s], ((s + j) % sp_count, t))
         for j in range(1, sp_count)
     ]
-    sends.append(remote(lat.at[t], lat.at[t], lat_send.at[2], lat_recv.at[2], (s, partner)))
-    pieces = (pl.ds(0, first), pl.ds(first, rows - first))
+    sends.append(remote(lat.at[t], lat.at[t], lat_send.at[6], lat_recv.at[6], (s, partner)))
+    pieces = [pl.ds(a, b - a) for a, b in zip(cuts, cuts[1:])]
     halves = [
         remote(lat.at[t, at], lat.at[t, at], lat_send.at[i], lat_recv.at[i], (s, across))
         for i, at in enumerate(pieces)
     ]
     for one in sends + halves[:1]:
         one.start()
+    def unit_rows(value):
+        value = value.astype(F32)
+        return value * lax.rsqrt(jnp.mean(value * value, axis=-1, keepdims=True) + NORM_EPS)
+
+    remote(lat.at[partner], lat.at[partner], lat_send.at[0], lat_recv.at[6], (s, partner)).wait_recv()
+    for i in range(2):
+        xs[i * rows : (i + 1) * rows, :] = unit_rows(lat[y * 2 + i])
     for j in range(1, sp_count):
         src = (s + j) % sp_count
         remote(part.at[src], part.at[src], part_send.at[0], part_recv.at[src], (s, partner)).wait_recv()
@@ -424,9 +430,21 @@
         remote(tot.at[t], tot.at[t], tot_send.at[j], tot_recv.at[t], (s, (t + j) % 4))
         for j in range(1, 4)
     ]
-    for one in last + halves[1:]:
+    ctx_rows = ctx.shape[1]
+    half = ctx_rows // 2
+    mine = pl.ds(pl.multiple_of(c * half, half), half)
+    yours = pl.ds(pl.multiple_of((1 - c) * half, half), half)
+    loads[5].wait()
+    raw = [
+        remote(
+            ctx.at[quad, mine], ctx.at[quad, mine], raw_send.at[0, n], raw_recv.at[0, quad],
+            ((((quad + n) % quads) * 2 + low) * 2 + x, t),
+        )
+        for n in range(1, quads)
+    ]
+    for one in last + halves[1:] + raw:
         one.start()
-    sends += last + halves
+    sends += last + halves + raw
     for j in range(1, 4):
         src = (t + j) % 4
         remote(tot.at[src], tot.at[src], tot_send.at[0], tot_recv.at[src], (s, partner)).wait_recv()
@@ -443,9 +461,7 @@
         one.start()
         sends.append(one)
 
-    def modulate(value, r):
-        value = value.astype(F32)
-        scaled = value * lax.rsqrt(jnp.mean(value * value, axis=-1, keepdims=True) + NORM_EPS)
+    def modulate(scaled, r):
         shift, scale = mod[r : r + 1, :width], mod[r : r + 1, width : 2 * width]
         return (scaled * (1.0 + scale) + shift).astype(BF16)
 
@@ -507,31 +523,22 @@
                             (to, y * 2 + target),
                         ))
 
-    def send_ctx(which, act):
-        for n in range(quads):
-            ok = allowed(n, which)
-            if ok is False:
-                continue
-            for i in range(2):
-                to, here = dest(i, n)
-
-                @pl.when(jnp.logical_not(here) & ok)
-                def _():
-                    act(remote(
-                        ckv.at[i], cb.at[z], c_send.at[n, i], c_recv.at[z], (to, y * 2 + target)
-                    ))
+    def send_ctx(act):
+        for i in range(2):
+            to, here = dest(i, 0)
+
+            @pl.when(jnp.logical_not(here))
+            def _():
+                act(remote(ckv.at[i], cb.at[low], c_send.at[i], c_recv.at[low], (to, y * 2 + target)))
 
     def pass_on(ph, act):
         spot = row_spot(1 - low)
         for n in range(1, quads):
             to = (((quad + n) % quads) * 2 + low) * 2 + x
-            if ph is None:
-                copies = [remote(cb.at[mate], cb.at[mate], pass_send.at[4, n], c_recv.at[mate], (to, t))]
-            else:
-                copies = [
-                    remote(ref, ref, pass_send.at[2 * ph + kind, n], kv_recv.at[kind, ph, mate], (to, t))
-                    for kind, ref in ((0, kb.at[quad, ph, spot]), (1, vb.at[quad, ph, :, spot]))
-                ]
+            copies = [
+                remote(ref, ref, pass_send.at[2 * ph + kind, n], kv_recv.at[kind, ph, mate], (to, t))
+                for kind, ref in ((0, kb.at[quad, ph, spot]), (1, vb.at[quad, ph, :, spot]))
+            ]
 
             @pl.when(free(n))
             def _():
@@ -567,10 +574,14 @@
     def start(one):
         one.start()
 
+    def sent(one):
+        one.wait_send()
+
     def project(ph):
         yy = (y + ph) % 2
         for i in range(2):
-            xn[i * rows : (i + 1) * rows, :] = modulate(lat[yy * 2 + i], 0)
+            at = slice(i * rows, (i + 1) * rows)
+            xn[at, :] = modulate(xs[at, :] if ph == 0 else unit_rows(lat[yy * 2 + i]), 0)
         value = xn[...]
         at = column(yy)
         cos, sin = cos_ref[:, :, at], sin_ref[:, :, at]
@@ -614,8 +625,7 @@
 
         if ph == 1:
             queries()
-            for which in ("early", "own", "late"):
-                send_ctx(which, start)
+            take_mate(0)
         keys()
         values()
         if ph == 0:
@@ -681,60 +691,66 @@
         axis=3,
     )
     acc[...] = jnp.zeros_like(acc)
-    for one in loads[2:]:
+    for one in loads[2:5] + loads[6:]:
         one.wait()
-    remote(lat.at[partner], lat.at[partner], lat_send.at[0], lat_recv.at[2], (s, partner)).wait_recv()
     project(0)
     relay_rows(0)
-    cn = modulate(ctx[...], 1)
-    kc = jnp.dot(cn, wk[...], preferred_element_type=F32)
-    vc = jnp.dot(cn, wv[...], preferred_element_type=F32)
-    for h in range(2):
-        ckv[h, 0] = unit(kc[:, h * head_dim : (h + 1) * head_dim], kgain).astype(BF16)
-        ckv[h, 1] = vc[:, h * head_dim : (h + 1) * head_dim].astype(BF16)
-
-    @pl.when(local)
-    def _():
-        cb[z] = ckv[x]
-
+    for n in range(1, quads):
+        ref = ctx.at[(quad + n) % quads, mine]
+        remote(ref, ref, raw_send.at[0, 0], raw_recv.at[0, (quad + n) % quads], (s, partner)).wait_recv()
+        one = remote(ref, ref, raw_send.at[1, n], raw_recv.at[1, (quad + n) % quads], (s, partner))
+        one.start()
+        sends.append(one)
     relay_rows(1)
-    take_mate(0)
+    relay_rows(2)
     other = (1 - y) * 2 + 1 - c
     for i, at in enumerate(pieces):
         ref = lat.at[other, at]
         remote(ref, ref, lat_send.at[0], lat_recv.at[3 + i], (s, partner)).wait_recv()
     project(1)
 
-    def sweep(ph, keys, values, bias):
-        count = keys().shape[0]
-
-        def stage_a(n):
-            score[n % 2, :count] = jnp.dot(keys(), qb[n // 2, ph, n % 2], preferred_element_type=F32)
-
-        def stage_b(n):
-            sc = score[n % 2, :count]
+    def sweep(ph, blocks, send=False):
+        tiles = [(block, n) for block in blocks for n in range(4)]
+
+        def stage_a(i):
+            (keys, _, _), n = tiles[i]
+            count = keys().shape[0]
+            score[i % 2, :count] = jnp.dot(keys(), qb[n // 2, ph, n % 2], preferred_element_type=F32)
+
+        def stage_b(i):
+            (keys, _, bias), n = tiles[i]
+            count = keys().shape[0]
+            sc = score[i % 2, :count]
             old = stat[ph, n // 2, n % 2, 0:1]
             new = jnp.maximum(old, jnp.max(sc, axis=0, keepdims=True) + bias)
             f = jnp.exp2(old - new)
-            fade[n % 2] = f
+            fade[i % 2] = f
             p = jnp.exp2(sc - (new - bias))
             stat[ph, n // 2, n % 2, 1:2] = (
                 stat[ph, n // 2, n % 2, 1:2] * f + jnp.sum(p, axis=0, keepdims=True)
             )
             stat[ph, n // 2, n % 2, 0:1] = new
-            prob[n % 2, :count] = p.astype(BF16)
-
-        def stage_c(n):
-            value = jnp.dot(values(), prob[n % 2, :count], preferred_element_type=F32)
-            acc[ph, n // 2, n % 2] = acc[ph, n // 2, n % 2] * fade[n % 2] + value
-
-        for n in range(6):
-            if n < 4:
-                stage_a(n)
-            if 1 <= n <= 4:
-                stage_b(n - 1)
-            if n >= 2:
-                stage_c(n - 2)
+            prob[i % 2, :count] = p.astype(BF16)
+
+        def stage_c(i):
+            (keys, values, _), n = tiles[i]
+            count = keys().shape[0]
+            value = jnp.dot(values(), prob[i % 2, :count], preferred_element_type=F32)
+            acc[ph, n // 2, n % 2] = acc[ph, n // 2, n % 2] * fade[i % 2] + value
+
+        for i in range(len(tiles) + 2):
+            if i < len(tiles):
+                stage_a(i)
+            if 1 <= i <= len(tiles):
+                stage_b(i - 1)
+            if i >= 2:
+                stage_c(i - 2)
+            if send and i == len(tiles) - 1:
+                for one in give(ph):
+                    one.start()
+
+    def latent(goal, late):
+        return (lambda: kb[goal, late], lambda: vb[goal, late], 0.0)
 
     def give(ph):
         return [
@@ -742,13 +758,28 @@
             remote(stat.at[ph, 0], stat_in.at[ph], s_send.at[ph], s_recv.at[ph], (s, partner)),
         ]
 
-    def have_ctx(goal):
+    def prefix():
+        for n in range(1, quads):
+            ref = ctx.at[(quad + n) % quads, yours]
+            remote(ref, ref, raw_send.at[0, 0], raw_recv.at[1, (quad + n) % quads], (s, partner)).wait_recv()
+        cn = jnp.concatenate([modulate(unit_rows(ctx[n]), 1) for n in range(quads)], axis=0)
+        kc = jnp.dot(cn, wk[...], preferred_element_type=F32)
+        vc = jnp.dot(cn, wv[...], preferred_element_type=F32)
+        for h in range(2):
+            ckv[h, 0] = unit(kc[:, h * head_dim : (h + 1) * head_dim], kgain).astype(BF16)
+            ckv[h, 1] = vc[:, h * head_dim : (h + 1) * head_dim].astype(BF16)
+        send_ctx(start)
+
+        @pl.when(local)
+        def _():
+            cb[low] = ckv[x]
+
+    def have_ctx():
         for lo in range(2):
-            k = goal * 2 + lo
-
-            @pl.when(jnp.logical_not(local & (k == z)))
+
+            @pl.when(jnp.logical_not(local & (lo == low)))
             def _():
-                remote(cb.at[k], cb.at[k], c_send.at[0, 0], c_recv.at[k], (s, partner)).wait_recv()
+                remote(cb.at[lo], cb.at[lo], c_send.at[0], c_recv.at[lo], (s, partner)).wait_recv()
 
     def sweeps(ph, late, begin, end, wait):
         def one(j, carry):
@@ -759,7 +790,7 @@
                 def _():
                     have_kv(goal, late)
 
-            sweep(ph, lambda: kb[goal, late], lambda: vb[goal, late], 0.0)
+            sweep(ph, [latent(goal, late)])
             return carry
 
         if end - begin == 1:
@@ -777,7 +808,7 @@
         @pl.when(jnp.logical_not(here))
         def _():
             act(remote(
-                ob.at[m, ph, mine], att.at[at, head], o_send.at[m, ph, cc],
+                ob.at[m, ph, mine], att.at[at, head], kv_send.at[m // 2, m % 2, ph, cc],
                 o_recv.at[x * 2 + c, ph, cc], (to, y * 2 + low),
             ))
 
@@ -801,8 +832,8 @@
                 den = 1.0 / (stat[ph, 1, pair, 1:2, lanes] * wa + stat_in[ph, pair, 1:2, lanes] * wb)
                 done = acc[ph, 1, pair, :, lanes] * (wa * den) + acc_in[ph, pair, :, lanes] * (wb * den)
                 ob[m, ph, cc * rows : (cc + 1) * rows] = done.T.astype(BF16)
-            for j in range(4):
-                return_o((place + 3 - j) % 4, ph, cc, start)
+            for m in (3 - place, (place + 2) % 4, place + 1 - 2 * x, place):
+                return_o(m, ph, cc, start)
 
     step_cols = width // chunks
 
@@ -814,7 +845,7 @@
 
     cores = [
         [
-            remote(core_out.at[h, n], core_in.at[h, n], core_send.at[h, n], core_recv.at[h, n], (s, partner))
+            remote(core_out.at[h, n], core_in.at[h, n], q_send.at[h, n // 2, n % 2], core_recv.at[h, n], (s, partner))
             for n in range(chunks)
         ]
         for h in range(2)
@@ -829,7 +860,7 @@
         for i in range(2):
             for g in range(2):
                 ref = att.at[at, pl.ds((i * 2 + g) * head_dim, head_dim)]
-                one = remote(ref, ref, o_send.at[0, 0, 0], o_recv.at[i * 2 + g, ph, cc], (s, partner))
+                one = remote(ref, ref, kv_send.at[0, 0, 0, 0], o_recv.at[i * 2 + g, ph, cc], (s, partner))
                 pl.when(jnp.logical_not(owner & (x == i) & (g == c)))(one.wait_recv)
 
     def mix(ph):
@@ -868,39 +899,33 @@
                 take_core(n, mixed[n])
 
     take_q(0)
+    prefix()
     have_q(0)
     have_own(0)
     sweeps(0, 0, 0, 1, False)
     sweeps(0, 0, 1, quads, True)
     take_q(1)
     have_q(1)
-    sweeps(1, 0, 0, 1, False)
-    have_ctx(quad)
-    pass_on(None, start)
     take_mate(1)
-    sweeps(1, 0, 1, quads, False)
+    sweep(1, [latent((quad + n) % quads, 0) for n in range(quads)])
     have_own(1)
-    sweeps(1, 1, 0, 1, False)
-    for n in range(1, quads):
-        have_ctx((quad + n) % quads)
-    ctx_keys = jnp.concatenate([cb[k, 0] for k in range(z_count)], axis=0)
-    ctx_values = jnp.concatenate([cb[k, 1] for k in range(z_count)], axis=0)
+    sweep(1, [latent(quad, 1)])
+    have_ctx()
+    ctx_keys = jnp.concatenate([cb[k, 0] for k in range(2)], axis=0)
+    ctx_values = jnp.concatenate([cb[k, 1] for k in range(2)], axis=0)
     ctx_values = ctx_values.astype(F32).T.astype(BF16)
-
-    def sweep_ctx(ph):
-        sweep(ph, lambda: ctx_keys, lambda: ctx_values, lift * math.log2(math.e))
-
-    sweep_ctx(1)
-    sweeps(1, 1, 1, quads, True)
-    for one in give(1):
-        one.start()
-    sweeps(0, 1, 0, 1, False)
+    ctx_block = (lambda: ctx_keys, lambda: ctx_values, lift * math.log2(math.e))
+    others = [(quad + n) % quads for n in range(1, quads)]
+    for goal in others:
+        have_kv(goal, 1)
+    sweep(1, [ctx_block] + [latent(goal, 1) for goal in others], send=True)
+    for ph in range(2):
+        send_kv(ph, (0, 1), "all", sent)
+        send_q(ph, sent)
     merge(1)
-    sweeps(0, 1, 1, quads, False)
-    sweep_ctx(0)
-    for one in give(0):
-        one.start()
+    sweep(0, [latent(quad, 1), ctx_block])
     mix(1)
+    sweep(0, [latent(goal, 1) for goal in others], send=True)
     merge(0)
     mix(0)
     square = jnp.zeros((rows, 1), F32)
@@ -915,20 +940,14 @@
         gate = mod[0:1, 2 * width + n * step_cols : 2 * width + (n + 1) * step_cols]
         out_ref[:, at] = (lat[t, :, at].astype(F32) + gate * (mixed[n] * inv)).astype(BF16)
 
-    def sent(one):
-        one.wait_send()
-
     for one in sends + give(0) + give(1) + cores[0] + cores[1] + mesh:
         one.wait_send()
     for ph in range(2):
-        send_kv(ph, (0, 1), "all", sent)
         pass_on(ph, sent)
-        send_q(ph, sent)
         for m in range(4):
             for cc in range(2):
                 return_o(m, ph, cc, sent)
-    send_ctx("all", sent)
-    pass_on(None, sent)
+    send_ctx(sent)
 
 
 def mix_kernel(
@@ -1050,7 +1069,7 @@
         DMA((6,)),
         pltpu.VMEM(mod_weight.shape, F32),
         pltpu.VMEM((4, rows, width), BF16),
-        pltpu.VMEM(context.shape, BF16),
+        pltpu.VMEM((quads, ctx_rows, width), BF16),
         pltpu.VMEM(query_weight.shape, BF16),
         pltpu.VMEM(key_matrix.shape, BF16),
         pltpu.VMEM(value_matrix.shape, BF16),
@@ -1061,14 +1080,15 @@
         pltpu.VMEM((4, 2, mod_cols), F32),
         pltpu.VMEM((2, 4 * mod_cols), F32),
         pltpu.VMEM((2 * rows, width), BF16),
+        pltpu.VMEM((2 * rows, width), F32),
         pltpu.VMEM((4, head_dim, all_rows), BF16),
         pltpu.VMEM((2, all_rows, head_dim), BF16),
         pltpu.VMEM((2, head_dim, all_rows), BF16),
-        pltpu.VMEM((2, 2, ctx_rows, head_dim), BF16),
+        pltpu.VMEM((2, 2, quads * ctx_rows, head_dim), BF16),
         pltpu.VMEM((2, 2, 2, head_dim, all_rows), BF16),
         pltpu.VMEM((quads, 2, all_rows, head_dim), BF16),
         pltpu.VMEM((quads, 2, head_dim, all_rows), BF16),
-        pltpu.VMEM((z_count, 2, ctx_rows, head_dim), BF16),
+        pltpu.VMEM((2, 2, quads * ctx_rows, head_dim), BF16),
         pltpu.VMEM((2, 2, 2, 2, all_rows), F32),
         pltpu.VMEM((2, 2, 2, head_dim, all_rows), F32),
         pltpu.VMEM((2, 2, 2, all_rows), F32),
@@ -1084,27 +1104,27 @@
         pltpu.VMEM((chunks, rows, step), BF16),
         pltpu.VMEM((chunks, rows, step), F32),
         DMA((7,)),
-        DMA((5,)),
-        DMA((5,)),
+        DMA((7,)),
+        DMA((7,)),
         DMA((sp_count,)),
         DMA((sp_count,)),
         DMA((4,)),
         DMA((4,)),
         DMA((2, 2, quads, 2)),
         DMA((2, 2, z_count)),
-        DMA((quads, 2)),
-        DMA((z_count,)),
+        DMA((2,)),
+        DMA((2,)),
         DMA((2, 2, 2)),
         DMA((2, 4, 2)),
         DMA((4, 2)),
-        DMA((5, quads)),
+        DMA((4, quads)),
+        DMA((2, quads)),
+        DMA((2, quads)),
         DMA((2,)),
         DMA((2,)),
         DMA((2,)),
         DMA((2,)),
         DMA((4, 2, 2)),
-        DMA((4, 2, 2)),
-        DMA((2, chunks)),
         DMA((2, chunks)),
         DMA((chunks,)),
         DMA((chunks,)),
@@ -1152,7 +1172,7 @@
         query_gain[None], key_gain[None],
     )
     wide = all_rows % GRID_W == 0 and all_rows == rows * 4 and rows % 128 == 0
-    if wide and kv_heads == 2 and group == 2 and x_count == 2 and sp_count % 4 == 0:
+    if wide and kv_heads == 2 and group == 2 and x_count == 2 and sp_count % 4 == 0 and ctx_rows % 32 == 0:
         return quad_call(args, out_weight, sp_count, head_dim, lift)
     chunks = 4
     y_count = tp_count // 2

time: 66.4 us -> 65.5 us (0.986)
  Pallas kernels: 65.4 us -> 64.5 us
    pallas_call x1, Pallas kernels: 65.4 us -> 64.5 us  [quad_call(): pl.pallas_call(functools.partial(quad_kernel, sp_count, head_dim, lift, c...]
where the time goes in v3:
time: 65.5 us; the launch traced here: 65.3 us
  Pallas kernels  64.5 us (98%)
  local copies, waits for them, and re-layouts  0.8 us (1%)
    pallas_call x1, Pallas kernels, quad_call(): pl.pallas_call(functools.partial(quad_kernel, sp_count, head_dim, lift, c...  64.5 us

profile of v3, /device:TPU:1, one launch (start us, length us, event | category | flops | bytes accessed | tf_op | source)
XLA Modules:
  0.0 65.3 jit_solution(2164797721022285100)
XLA Ops:
  0.0 64.5 %quad.1 = bf16[128,2048]{1,0:T(8,128)(2,1)S(1)} custom-call(f32[1,256]{1,0:T(1,128)} %bitcast.4, f32[1,256]{1,0:T(1,128)} %bitcast.5, f32[256,1536]{1,0:T(8,128)} %refs_2_.1, bf16[128,2048]{1,0:T(8,128)(2,1)} %refs_3_.1, bf16[64,2048]{1,0:T(8,128)(2,1)} %refs_4_.1, bf16[2048,512]{1,0:T(8,128)(2,1)} %refs_5_.1, bf16[2048,256]{1,0:T(8,128)(2,1)} %refs_6_.1, ...), custom_call_target="tpu_custom_call" | custom-call | tf_op jit(solution)/shard_map/quad/pallas_call | solution.py:1132
  64.5 0.8 %copy.15 = bf16[128,2048]{1,0:T(8,128)(2,1)} copy(bf16[128,2048]{1,0:T(8,128)(2,1)S(1)} %quad.1) | data formatting | bytes 1048576

commit v4 on v3

--- a/solution.py
+++ b/solution.py
@@ -546,28 +546,28 @@
                     act(one)
 
     def spot_of(m):
-        return m // 2, pl.ds(pl.multiple_of(m % 2 * span, span), span)
+        return pl.ds(pl.multiple_of(m * rows, rows), rows)
 
     def send_q(ph, act):
-        at = column((y + ph) % 2)
-        pair, lanes = spot_of(place)
+        blocks = pl.ds((y + ph) % 2 * 2, 2)
+        lanes = spot_of(place)
         for i in range(2):
             to = (quad * 2 + c) * 2 + i
             for g in range(2):
                 mine = (to == s) & (g == c)
-                src = qt.at[i * 2 + g, :, at]
+                src = qt.at[i * 2 + g, blocks]
 
                 @pl.when(mine)
                 def _():
                     act(remote(
-                        src, qb.at[0, ph, pair, :, lanes], q_send.at[ph, i, g],
+                        src, qb.at[0, ph, :, :, lanes], q_send.at[ph, i, g],
                         q_recv.at[0, place, ph], (s, partner),
                     ))
 
                 @pl.when(jnp.logical_not(mine))
                 def _():
                     act(remote(
-                        src, qb.at[1, ph, pair, :, lanes], q_send.at[ph, i, g],
+                        src, qb.at[1, ph, :, :, lanes], q_send.at[ph, i, g],
                         q_recv.at[1, place, ph], (to, y * 2 + g),
                     ))
 
@@ -614,14 +614,17 @@
                         value, wq[:, h * head_dim : (h + 2) * head_dim], preferred_element_type=F32
                     )
                 yh = full[:, (h % 2) * head_dim : (h % 2 + 1) * head_dim]
-                qt[h, :, at] = turn(unit(yh, qgain).T, cos, sin).astype(BF16)
+                turned = turn(unit(yh, qgain).T, cos, sin).astype(BF16)
+                for cc in range(2):
+                    qt[h, yy * 2 + cc] = turned[:, cc * rows : (cc + 1) * rows]
             send_q(ph, start)
-            pair, lanes = spot_of(place)
+            lanes = spot_of(place)
 
             @pl.when(owner)
             def _():
-                qb[1, ph, pair, :, lanes] = qt[x * 2 + c, :, at]
-                qb[0, ph, pair, :, lanes] = qt[x * 2 + 1 - c, :, at]
+                for cc in range(2):
+                    qb[1, ph, cc, :, lanes] = qt[x * 2 + c, yy * 2 + cc]
+                    qb[0, ph, cc, :, lanes] = qt[x * 2 + 1 - c, yy * 2 + cc]
 
         if ph == 1:
             queries()
@@ -635,11 +638,11 @@
     def take_q(ph):
         for j in range(1, 4):
             m = (place + j) % 4
-            pair, lanes = spot_of(m)
-            ref = qb.at[1, ph, pair, :, lanes]
+            lanes = spot_of(m)
+            ref = qb.at[1, ph, :, :, lanes]
             remote(ref, ref, relay_send.at[0, 0], q_recv.at[1, m, ph], (s, partner)).wait_recv()
             one = remote(
-                ref, qb.at[0, ph, pair, :, lanes], relay_send.at[j, ph], q_recv.at[0, m, ph],
+                ref, qb.at[0, ph, :, :, lanes], relay_send.at[j, ph], q_recv.at[0, m, ph],
                 (s, partner),
             )
             one.start()
@@ -648,9 +651,9 @@
     def have_q(ph):
         for j in range(4):
             m = (place + j) % 4
-            pair, lanes = spot_of(m)
+            lanes = spot_of(m)
             for role in range(2) if j == 0 else range(1):
-                ref = qb.at[role, ph, pair, :, lanes]
+                ref = qb.at[role, ph, :, :, lanes]
                 one = remote(ref, ref, relay_send.at[0, 0], q_recv.at[role, m, ph], (s, partner))
                 if j == 0:
                     pl.when(jnp.logical_not(owner))(one.wait_recv)
@@ -715,28 +718,28 @@
         def stage_a(i):
             (keys, _, _), n = tiles[i]
             count = keys().shape[0]
-            score[i % 2, :count] = jnp.dot(keys(), qb[n // 2, ph, n % 2], preferred_element_type=F32)
+            score[i % 2, :count] = jnp.dot(keys(), qb[n % 2, ph, n // 2], preferred_element_type=F32)
 
         def stage_b(i):
             (keys, _, bias), n = tiles[i]
             count = keys().shape[0]
             sc = score[i % 2, :count]
-            old = stat[ph, n // 2, n % 2, 0:1]
+            old = stat[ph, n % 2, n // 2, 0:1]
             new = jnp.maximum(old, jnp.max(sc, axis=0, keepdims=True) + bias)
             f = jnp.exp2(old - new)
             fade[i % 2] = f
             p = jnp.exp2(sc - (new - bias))
-            stat[ph, n // 2, n % 2, 1:2] = (
-                stat[ph, n // 2, n % 2, 1:2] * f + jnp.sum(p, axis=0, keepdims=True)
+            stat[ph, n % 2, n // 2, 1:2] = (
+                stat[ph, n % 2, n // 2, 1:2] * f + jnp.sum(p, axis=0, keepdims=True)
             )
-            stat[ph, n // 2, n % 2, 0:1] = new
+            stat[ph, n % 2, n // 2, 0:1] = new
             prob[i % 2, :count] = p.astype(BF16)
 
         def stage_c(i):
             (keys, values, _), n = tiles[i]
             count = keys().shape[0]
             value = jnp.dot(values(), prob[i % 2, :count], preferred_element_type=F32)
-            acc[ph, n // 2, n % 2] = acc[ph, n // 2, n % 2] * fade[i % 2] + value
+            acc[ph, n % 2, n // 2] = acc[ph, n % 2, n // 2] * fade[i % 2] + value
 
         for i in range(len(tiles) + 2):
             if i < len(tiles):
@@ -745,17 +748,17 @@
                 stage_b(i - 1)
             if i >= 2:
                 stage_c(i - 2)
-            if send and i == len(tiles) - 1:
-                for one in give(ph):
+            if send and i >= len(tiles) - 2 and (len(tiles) - i) % 2 == 0:
+                for one in give(ph, 0 if i < len(tiles) else 1):
                     one.start()
 
     def latent(goal, late):
         return (lambda: kb[goal, late], lambda: vb[goal, late], 0.0)
 
-    def give(ph):
+    def give(ph, cc):
         return [
-            remote(acc.at[ph, 0], acc_in.at[ph], a_send.at[ph], a_recv.at[ph], (s, partner)),
-            remote(stat.at[ph, 0], stat_in.at[ph], s_send.at[ph], s_recv.at[ph], (s, partner)),
+            remote(acc.at[ph, 0, cc], acc_in.at[ph, cc], a_send.at[ph, cc], a_recv.at[ph, cc], (s, partner)),
+            remote(stat.at[ph, 0, cc], stat_in.at[ph, cc], s_send.at[ph, cc], s_recv.at[ph, cc], (s, partner)),
         ]
 
     def prefix():
@@ -819,18 +822,16 @@
                 att[at, head] = ob[m, ph, mine]
 
     def merge(ph):
-        for one in give(ph):
-            one.wait_recv()
         for cc in range(2):
-            for j in range(4):
-                m = (place + 3 - j) % 4
-                pair, half = m // 2, m % 2
-                lanes = pl.ds(pl.multiple_of(half * span + cc * rows, rows), rows)
-                a, b = stat[ph, 1, pair, 0:1, lanes], stat_in[ph, pair, 0:1, lanes]
+            for one in give(ph, cc):
+                one.wait_recv()
+            for m in range(4):
+                lanes = slice(m * rows, (m + 1) * rows)
+                a, b = stat[ph, 1, cc, 0:1, lanes], stat_in[ph, cc, 0:1, lanes]
                 peak = jnp.maximum(a, b)
                 wa, wb = jnp.exp2(a - peak), jnp.exp2(b - peak)
-                den = 1.0 / (stat[ph, 1, pair, 1:2, lanes] * wa + stat_in[ph, pair, 1:2, lanes] * wb)
-                done = acc[ph, 1, pair, :, lanes] * (wa * den) + acc_in[ph, pair, :, lanes] * (wb * den)
+                den = 1.0 / (stat[ph, 1, cc, 1:2, lanes] * wa + stat_in[ph, cc, 1:2, lanes] * wb)
+                done = acc[ph, 1, cc, :, lanes] * (wa * den) + acc_in[ph, cc, :, lanes] * (wb * den)
                 ob[m, ph, cc * rows : (cc + 1) * rows] = done.T.astype(BF16)
             for m in (3 - place, (place + 2) % 4, place + 1 - 2 * x, place):
                 return_o(m, ph, cc, start)
@@ -863,11 +864,11 @@
                 one = remote(ref, ref, kv_send.at[0, 0, 0, 0], o_recv.at[i * 2 + g, ph, cc], (s, partner))
                 pl.when(jnp.logical_not(owner & (x == i) & (g == c)))(one.wait_recv)
 
-    def mix(ph):
+    def mix(ph, cc):
         yy = (y + ph) % 2
 
-        def give_core(cc, n):
-            core_out[ph, n] = piece(n, yy, cc).astype(BF16)
+        def give_core(block, n):
+            core_out[ph, n] = piece(n, yy, block).astype(BF16)
             cores[ph][n].start()
 
         def take_core(n, value):
@@ -879,24 +880,31 @@
             else:
                 mixed[n] = value
 
-        have_o(ph, 0)
-
-        @pl.when(c == 1)
+        if cc == 0:
+            have_o(ph, 0)
+
+            @pl.when(c == 1)
+            def _():
+                for n in range(chunks):
+                    give_core(0, n)
+
+            @pl.when(c == 0)
+            def _():
+                for n in range(chunks):
+                    mixed[n] = piece(n, yy, 0)
+                for n in range(chunks):
+                    take_core(n, mixed[n])
+
+            return
+
+        @pl.when(c == (0 if cc == 1 else 1))
         def _():
-            for n in range(chunks):
-                give_core(0, n)
             have_o(ph, 1)
             for n in range(chunks):
+                if cc == 1:
+                    give_core(1, n)
+                    continue
                 take_core(n, piece(n, yy, 1))
-
-        @pl.when(c == 0)
-        def _():
-            for n in range(chunks):
-                mixed[n] = piece(n, yy, 0)
-            have_o(ph, 1)
-            for n in range(chunks):
-                give_core(1, n)
-                take_core(n, mixed[n])
 
     take_q(0)
     prefix()
@@ -910,24 +918,29 @@
     sweep(1, [latent((quad + n) % quads, 0) for n in range(quads)])
     have_own(1)
     sweep(1, [latent(quad, 1)])
+    others = [(quad + n) % quads for n in range(1, quads)]
+    for goal in others:
+        have_kv(goal, 1)
+    sweep(1, [latent(goal, 1) for goal in others])
     have_ctx()
     ctx_keys = jnp.concatenate([cb[k, 0] for k in range(2)], axis=0)
     ctx_values = jnp.concatenate([cb[k, 1] for k in range(2)], axis=0)
     ctx_values = ctx_values.astype(F32).T.astype(BF16)
     ctx_block = (lambda: ctx_keys, lambda: ctx_values, lift * math.log2(math.e))
-    others = [(quad + n) % quads for n in range(1, quads)]
-    for goal in others:
-        have_kv(goal, 1)
-    sweep(1, [ctx_block] + [latent(goal, 1) for goal in others], send=True)
+    sweep(1, [ctx_block], send=True)
     for ph in range(2):
         send_kv(ph, (0, 1), "all", sent)
         send_q(ph, sent)
     merge(1)
     sweep(0, [latent(quad, 1), ctx_block])
-    mix(1)
+    mix(1, 0)
+    mix(1, 1)
     sweep(0, [latent(goal, 1) for goal in others], send=True)
+    mix(1, 2)
     merge(0)
-    mix(0)
+    mix(0, 0)
+    mix(0, 1)
+    mix(0, 2)
     square = jnp.zeros((rows, 1), F32)
     for n in range(chunks):
         mesh[n].wait_recv()
@@ -940,7 +953,8 @@
         gate = mod[0:1, 2 * width + n * step_cols : 2 * width + (n + 1) * step_cols]
         out_ref[:, at] = (lat[t, :, at].astype(F32) + gate * (mixed[n] * inv)).astype(BF16)
 
-    for one in sends + give(0) + give(1) + cores[0] + cores[1] + mesh:
+    given = [one for ph in range(2) for cc in range(2) for one in give(ph, cc)]
+    for one in sends + given + cores[0] + cores[1] + mesh:
         one.wait_send()
     for ph in range(2):
         pass_on(ph, sent)
@@ -1081,7 +1095,7 @@
         pltpu.VMEM((2, 4 * mod_cols), F32),
         pltpu.VMEM((2 * rows, width), BF16),
         pltpu.VMEM((2 * rows, width), F32),
-        pltpu.VMEM((4, head_dim, all_rows), BF16),
+        pltpu.VMEM((4, 4, head_dim, rows), BF16),
         pltpu.VMEM((2, all_rows, head_dim), BF16),
         pltpu.VMEM((2, head_dim, all_rows), BF16),
         pltpu.VMEM((2, 2, quads * ctx_rows, head_dim), BF16),
@@ -1120,10 +1134,10 @@
         DMA((4, quads)),
         DMA((2, quads)),
         DMA((2, quads)),
-        DMA((2,)),
-        DMA((2,)),
-        DMA((2,)),
-        DMA((2,)),
+        DMA((2, 2)),
+        DMA((2, 2)),
+        DMA((2, 2)),
+        DMA((2, 2)),
         DMA((4, 2, 2)),
         DMA((2, chunks)),
         DMA((chunks,)),

time: 65.5 us -> 65.1 us (level)
  no operation moved by 1% of the time
where the time goes in v4:
time: 65.1 us; the launch traced here: 64.9 us
  Pallas kernels  64.1 us (98%)
  local copies, waits for them, and re-layouts  0.8 us (1%)
    pallas_call x1, Pallas kernels, quad_call(): pl.pallas_call(functools.partial(quad_kernel, sp_count, head_dim, lift, c...  64.1 us

profile of v4, /device:TPU:1, one launch (start us, length us, event | category | flops | bytes accessed | tf_op | source)
XLA Modules:
  0.0 64.9 jit_solution(7187427213255979981)
XLA Ops:
  0.0 64.1 %quad.1 = bf16[128,2048]{1,0:T(8,128)(2,1)S(1)} custom-call(f32[1,256]{1,0:T(1,128)} %bitcast.4, f32[1,256]{1,0:T(1,128)} %bitcast.5, f32[256,1536]{1,0:T(8,128)} %refs_2_.1, bf16[128,2048]{1,0:T(8,128)(2,1)} %refs_3_.1, bf16[64,2048]{1,0:T(8,128)(2,1)} %refs_4_.1, bf16[2048,512]{1,0:T(8,128)(2,1)} %refs_5_.1, bf16[2048,256]{1,0:T(8,128)(2,1)} %refs_6_.1, ...), custom_call_target="tpu_custom_call" | custom-call | tf_op jit(solution)/shard_map/quad/pallas_call | solution.py:1146
  64.1 0.8 %copy.15 = bf16[128,2048]{1,0:T(8,128)(2,1)} copy(bf16[128,2048]{1,0:T(8,128)(2,1)S(1)} %quad.1) | data formatting | bytes 1048576

commit v5 on v4

--- a/solution.py
+++ b/solution.py
@@ -932,10 +932,10 @@
         send_kv(ph, (0, 1), "all", sent)
         send_q(ph, sent)
     merge(1)
-    sweep(0, [latent(quad, 1), ctx_block])
+    sweep(0, [latent(quad, 1)])
     mix(1, 0)
     mix(1, 1)
-    sweep(0, [latent(goal, 1) for goal in others], send=True)
+    sweep(0, [ctx_block] + [latent(goal, 1) for goal in others], send=True)
     mix(1, 2)
     merge(0)
     mix(0, 0)

time: 65.1 us -> 65.1 us (level)
  no operation moved by 1% of the time
where the time goes in v5:
time: 65.1 us; the launch traced here: 64.9 us
  Pallas kernels  64.1 us (98%)
  local copies, waits for them, and re-layouts  0.8 us (1%)
    pallas_call x1, Pallas kernels, quad_call(): pl.pallas_call(functools.partial(quad_kernel, sp_count, head_dim, lift, c...  64.1 us

profile of v5, /device:TPU:1, one launch (start us, length us, event | category | flops | bytes accessed | tf_op | source)
XLA Modules:
  0.0 64.9 jit_solution(5682609724352427147)
XLA Ops:
  0.0 64.1 %quad.1 = bf16[128,2048]{1,0:T(8,128)(2,1)S(1)} custom-call(f32[1,256]{1,0:T(1,128)} %bitcast.4, f32[1,256]{1,0:T(1,128)} %bitcast.5, f32[256,1536]{1,0:T(8,128)} %refs_2_.1, bf16[128,2048]{1,0:T(8,128)(2,1)} %refs_3_.1, bf16[64,2048]{1,0:T(8,128)(2,1)} %refs_4_.1, bf16[2048,512]{1,0:T(8,128)(2,1)} %refs_5_.1, bf16[2048,256]{1,0:T(8,128)(2,1)} %refs_6_.1, ...), custom_call_target="tpu_custom_call" | custom-call | tf_op jit(solution)/shard_map/quad/pallas_call | solution.py:1146
  64.1 0.8 %copy.15 = bf16[128,2048]{1,0:T(8,128)(2,1)} copy(bf16[128,2048]{1,0:T(8,128)(2,1)S(1)} %quad.1) | data formatting | bytes 1048576
